TPU v7x, 32 devices: a whole 2x2x4 slice. The times are simulated.
32 devices in a mesh: rep: 2 (over y), fs: 4 (over z), tp: 4 (over x, core).
Axes of the slice: x: 2, y: 2, z: 4, core: 2. Of those that a mesh axis runs over, the one named last changes fastest.
Arguments:
- tokens: bfloat16 [2048, 2048], P(('rep', 'fs')), may hold values from -6 to 6
- gate_weight: bfloat16 [2048, 2816], P('fs', 'tp'), may hold values from -0.125 to 0.125
- up_weight: bfloat16 [2048, 2816], P('fs', 'tp'), may hold values from -0.125 to 0.125
- down_weight: bfloat16 [2816, 2048], P('tp', 'fs'), may hold values from -0.109375 to 0.109375
- out_grad: bfloat16 [2048, 2048], P(('rep', 'fs')), may hold values from -6 to 6
Outputs:
- input_grad: bfloat16 [2048, 2048], P(('rep', 'fs'))
- down_grad: float32 [2816, 2048], P('tp', 'fs')
- row_norms: float32 [2816], P('tp')
All inputs are finite; a program needn't handle non-finite values.
Results may differ from a plain program's by a relative error of at most 0.024.
Values may be sent and summed in bfloat16 or wider, within the bound.
A program may use at most 64 MiB of HBM per device.

v0:
```python
import functools

import jax
import jax.numpy as jnp
from jax import lax
from jax.experimental import pallas as pl
from jax.experimental.pallas import tpu as pltpu
from jax.sharding import PartitionSpec as P

MESH = pl.DeviceIdType.MESH
BF16 = jnp.bfloat16
F32 = jnp.float32


def contract_last(left, right):
    return lax.dot_general(left, right, (((1,), (1,)), ((), ())), preferred_element_type=F32)


def contract_first(left, right):
    return lax.dot_general(left, right, (((0,), (0,)), ((), ())), preferred_element_type=F32)


def block_kernel(
    n, gate, up, down, tokens, grad, input_grad, down_grad, norms,
    gate_all, up_all, down_all, tokens_all, grad_all,
    gate_pre, up_pre, hid, gate_grad, up_grad, part, p_in, p_out,
    f_out, f_in, g_own, g_out, g_in, h_out, h_in, whole_out, s_own, s_other, n_own, n_in,
    w_send, w_recv, p_send, p_recv, pair_send, pair_recv, own_sem, g_send, g_recv,
    s_send, s_recv, n_send, n_recv,
):
    f = lax.axis_index("fs")
    r = lax.axis_index("rep")
    t = lax.axis_index("tp")
    c, x = lax.rem(t, 2), t // 2
    mate, far = {"tp": x * 2 + 1 - c}, {"tp": (1 - x) * 2 + c}
    pair = {"rep": 1 - r}
    rows, depth = tokens.shape
    units, width = gate.shape
    half, strip = depth // 2, width // 2
    pieces = g_out.shape[0]
    size = half // pieces
    down_half = down.at[pl.ds(pl.multiple_of(r * units, 16), units)]

    barrier = pltpu.get_barrier_semaphore()
    peers = [{"rep": lax.rem(r + a, 2), "fs": lax.rem(f + k, n)}
             for a in range(2) for k in range(n) if a or k]
    for peer in peers + [mate, far]:
        pl.semaphore_signal(barrier, inc=1, device_id=peer, device_id_type=MESH)
    pl.semaphore_wait(barrier, 2 * n + 1)

    def cols(start, size):
        return pl.ds(pl.multiple_of(start, size), size)

    def remote(src, dst, send, recv, peer):
        return pltpu.make_async_remote_copy(
            src_ref=src, dst_ref=dst, send_sem=send, recv_sem=recv,
            device_id=peer, device_id_type=MESH,
        )

    shards = ((gate, gate_all), (up, up_all), (down_half, down_all))
    ways = (1, 0)

    def hop(w, step, way, arriving=False):
        own, whole = shards[w]
        sign = 1 if way else -1
        owner = f - sign * (step + 1 if arriving else step)
        place = whole.at[:, cols(owner * width, width)]
        return remote(
            own if step == 0 and not arriving else place, place,
            w_send.at[way, w, step], w_recv.at[way, w, step],
            {"fs": f - sign if arriving else f + sign},
        )

    def sends(step, way):
        return (f < n - 1) & (f >= step) if way else (f > 0) & (f + step <= n - 1)

    def receives(step, way):
        return f - 1 - step >= 0 if way else f + 1 + step <= n - 1

    def forward(w, step):
        for way in ways:
            @pl.when(sends(step, way))
            def _():
                hop(w, step, way).start()

    def arrive(w, step):
        for way in ways:
            @pl.when(receives(step, way))
            def _():
                hop(w, step, way, True).wait_recv()

    for w in range(2):
        forward(w, 0)
    pairs = []
    for i, (own, whole) in enumerate(((tokens, tokens_all), (grad, grad_all))):
        copy = remote(own, whole.at[pl.ds(rows, rows)], pair_send.at[i], pair_recv.at[i], pair)
        copy.start()
        pairs.append(copy)
    local = []
    for i, (own, place) in enumerate((
        (tokens, tokens_all.at[pl.ds(0, rows)]),
        (grad, grad_all.at[pl.ds(0, rows)]),
        (gate, gate_all.at[:, cols(f * width, width)]),
        (up, up_all.at[:, cols(f * width, width)]),
        (down_half, down_all.at[:, cols(f * width, width)]),
    )):
        copy = pltpu.make_async_copy(own, place, own_sem.at[i])
        copy.start()
        local.append(copy)

    for step in range(n - 1):
        if step == n - 2:
            forward(2, 0)
        for w in range(2):
            arrive(w, step)
            if step + 1 < n - 1:
                forward(w, step + 1)
    for copy in pairs + local:
        copy.wait()

    for b in range(2):
        span = pl.ds(b * rows, rows)
        gate_pre[span] = contract_last(tokens_all[span], gate_all[...])
        up_pre[span] = contract_last(tokens_all[span], up_all[...])

    def relay_down(step):
        arrive(2, step)
        if step + 1 < n - 1:
            forward(2, step + 1)

    relay_down(0)
    pre, raw = gate_pre[...], up_pre[...]
    sigma = jax.nn.sigmoid(pre)
    hidden = (pre * sigma * raw).astype(BF16)
    gate_pre[...] = pre * sigma
    up_pre[...] = raw * sigma * (1.0 + pre * (1.0 - sigma))
    for k in range(n):
        at = pl.ds(k * width, width)
        part[:, at] = contract_first(hidden, grad_all[:, at]).astype(BF16)

    def sum_goes(step, way):
        return f <= n - 2 - step if way else f >= step + 1

    def sum_comes(step, way):
        return (f >= 1) & (f <= n - 1 - step) if way else (f <= n - 2) & (f >= step)

    def lanes(k, base=0):
        return pl.ds(base * width + k * strip, strip)

    def sum_copy(step, way, k, first):
        target = n - 1 - step if way else step
        return remote(
            part.at[:, lanes(k, target)] if first else p_out.at[way, step, :, lanes(k)],
            p_in.at[way, step, :, lanes(k)], p_send.at[way, step, k], p_recv.at[way, step, k],
            {"fs": f + 1 if way else f - 1},
        )

    def at_end(way):
        return f == 0 if way else f == n - 1

    for step in range(n - 1):
        for way in ways:
            @pl.when(at_end(way))
            def _():
                for k in range(2):
                    sum_copy(step, way, k, True).start()

    def relay_sum(step, hops, k):
        for way in ways:
            target = n - 1 - step if way else step
            here = f == hops if way else f == n - 1 - hops

            @pl.when(sum_comes(step, way) & here)
            def _():
                sum_copy(step, way, k, False).wait_recv()

            @pl.when(sum_comes(step, way) & sum_goes(step, way) & here)
            def _():
                p_out[way, step, :, lanes(k)] = (
                    part[:, lanes(k, target)].astype(F32) + p_in[way, step, :, lanes(k)].astype(F32)
                ).astype(BF16)
                sum_copy(step, way, k, False).start()

    def relay_sums(when, k):
        for step in range(n - 1):
            hops = when - step
            if 1 <= hops <= n - 1 - step:
                relay_sum(step, hops, k)

    def add_shard(owner):
        at = cols(owner * width, width)
        hid[...] += contract_last(grad_all[:, at], down_all[:, at])

    def add_shards(step):
        for way in ways:
            @pl.when(receives(step, way))
            def _():
                add_shard(f - 1 - step if way else f + 1 + step)

    mine = cols(f * width, width)
    hid[...] = contract_last(grad_all[:, mine], down_all[:, mine])
    add_shards(0)
    for step in range(1, n - 1):
        relay_down(step)
        add_shards(step)
        if step == 1:
            relay_sums(1, 0)
            relay_sums(1, 1)
    if n == 2:
        relay_sums(1, 0)
        relay_sums(1, 1)

    for b in range(2):
        span = pl.ds(b * rows, rows)
        up_grad[span] = (hid[span] * gate_pre[span]).astype(BF16)
        gate_grad[span] = (hid[span] * up_pre[span]).astype(BF16)

    def flow(b, at):
        span = pl.ds(b * rows, rows)
        return (
            jnp.dot(gate_grad[span], gate_all[:, at], preferred_element_type=F32)
            + jnp.dot(up_grad[span], up_all[:, at], preferred_element_type=F32)
        )

    def push(i, src, dst, peer):
        copy = remote(src, dst, g_send.at[i], g_recv.at[i], peer)
        copy.start()
        return copy

    cross = {}
    for b in (1, 0):
        f_out[b] = flow(b, cols((1 - c) * half, half)).astype(BF16)
        cross[b] = push(b, f_out.at[b], f_in.at[b], mate)
    over = []
    for b in (1, 0):
        if b == 0:
            for k in range(2):
                relay_sums(2, k)
        kept = flow(b, cols(c * half, half))
        cross[b].wait()
        kept = kept + f_in[b].astype(F32)
        for q in range(pieces):
            piece = kept[:, q * size:(q + 1) * size]
            if b == 1:
                g_out[q] = piece.astype(BF16)
                over.append(push(2 + q, g_out.at[q], g_in.at[q], pair))
            else:
                g_own[q] = piece
    across = []
    for q in range(pieces):
        over[q].wait()
        h_out[q] = (g_own[q] + g_in[q].astype(F32)).astype(BF16)
        across.append(push(2 + pieces + q, h_out.at[q], h_in.at[q], far))
    swaps = []
    for k in range(2):
        for when in range(3, n):
            relay_sums(when, k)

        def finish(way):
            step = n - 1 - f if way else f
            return p_in[way, lax.rem(step, n - 1), :, lanes(k)].astype(F32)

        at = pl.ds(pl.multiple_of(f * width + k * strip, strip), strip)
        s_sum = part[:, at].astype(F32)
        s_sum = s_sum + jnp.where(f > 0, finish(1), 0.0) + jnp.where(f < n - 1, finish(0), 0.0)
        s_own[:, lanes(k)] = s_sum.astype(BF16)
        copy = remote(
            s_own.at[:, lanes(k)], s_other.at[:, lanes(k)], s_send.at[k], s_recv.at[k], pair
        )
        copy.start()
        swaps.append(copy)
    kept = s_own[...].astype(F32)
    down_grad[pl.ds(pl.multiple_of(r * units, 16), units), :] = s_own[...]
    n_own[...] = lax.dot_general(
        jnp.ones((8, width), F32), kept * kept, (((1,), (1,)), ((), ())),
        precision=lax.Precision.HIGHEST, preferred_element_type=F32,
    )
    small = []
    for i, peer in enumerate(peers):
        copy = remote(n_own, n_in.at[i], n_send.at[i], n_recv.at[i], peer)
        copy.start()
        small.append(copy)
    beside = []
    for q in range(pieces):
        across[q].wait()
        at = cols(c * half + q * size, size)
        whole_out[:, at] = (h_out[q].astype(F32) + h_in[q].astype(F32)).astype(BF16)
        beside.append(push(2 + 2 * pieces + q, whole_out.at[:, at], whole_out.at[:, at], mate))
    for step in range(n - 1):
        for way in ways:
            for w in range(3):
                @pl.when(sends(step, way))
                def _():
                    hop(w, step, way).wait_send()

            @pl.when(sum_goes(step, way))
            def _():
                for k in range(2):
                    sum_copy(step, way, k, False).wait_send()
    for copy in small:
        copy.wait()
    here = n_own[...]
    for i in range(n - 1):
        here = here + n_in[i]
    there = n_in[n - 1]
    for i in range(n, 2 * n - 1):
        there = there + n_in[i]
    norms[...] = jnp.concatenate(
        [jnp.where(r == 0, here, there), jnp.where(r == 0, there, here)], axis=1
    )
    for copy in swaps:
        copy.wait()
    down_grad[pl.ds(pl.multiple_of((1 - r) * units, 16), units), :] = s_other[...]
    for copy in beside:
        copy.wait()
    input_grad[...] = whole_out[...]


def write_kernel(flow, shard, rows, input_grad, down_grad, norms):
    input_grad[...] = flow[...]
    down_grad[...] = shard[...].astype(F32)
    norms[...] = rows[0]


def split_units(n, tokens, gate_weight, up_weight, down_weight, out_grad):
    rows, depth = tokens.shape
    width, both = gate_weight.shape
    units = both // 2
    start = lax.axis_index("rep") * units
    gate = lax.dynamic_slice_in_dim(gate_weight, start, units, 1).T
    up = lax.dynamic_slice_in_dim(up_weight, start, units, 1).T
    anywhere = pl.BlockSpec(memory_space=pl.ANY)
    vmem = pl.BlockSpec(memory_space=pltpu.VMEM)
    dma = pltpu.SemaphoreType.DMA
    half, pieces = depth // 2, 4
    piece = (pieces, rows, half // pieces)
    peers = 2 * n - 1
    scratch = [((units, depth), BF16)] * 3 + [((2 * rows, depth), BF16)] * 2
    scratch += [((2 * rows, units), F32)] * 3 + [((2 * rows, units), BF16)] * 2
    scratch += [((units, depth), BF16)] + [((2, n - 1, units, width), BF16)] * 2
    scratch += [((2, rows, half), BF16)] * 2 + [(piece, F32)] + [(piece, BF16)] * 4
    scratch += [((rows, depth), BF16)] + [((units, width), BF16)] * 2
    scratch += [((8, units), F32), ((peers, 8, units), F32)]
    input_grad, down_grad, norms = pl.pallas_call(
        functools.partial(block_kernel, n),
        out_shape=[
            jax.ShapeDtypeStruct((rows, depth), BF16),
            jax.ShapeDtypeStruct((both, width), BF16),
            jax.ShapeDtypeStruct((8, both), F32),
        ],
        in_specs=[vmem] * 2 + [anywhere] * 3,
        out_specs=[vmem] * 3,
        scratch_shapes=[pltpu.VMEM(shape, kind) for shape, kind in scratch] + [
            dma((2, 3, n - 1)), dma((2, 3, n - 1)), dma((2, n - 1, 2)), dma((2, n - 1, 2)),
            dma((2,)), dma((2,)), dma((5,)), dma((2 + 3 * pieces,)), dma((2 + 3 * pieces,)),
            dma((2,)), dma((2,)), dma((peers,)), dma((peers,)),
        ],
        compiler_params=pltpu.CompilerParams(collective_id=0, has_side_effects=True),
        name="block",
    )(gate, up, down_weight, tokens, out_grad)
    return tuple(pl.pallas_call(
        write_kernel,
        out_shape=[
            jax.ShapeDtypeStruct((rows, depth), BF16),
            jax.ShapeDtypeStruct((both, width), F32),
            jax.ShapeDtypeStruct((both,), F32),
        ],
        in_specs=[vmem] * 3,
        out_specs=[vmem] * 3,
        name="write",
    )(input_grad, down_grad, norms))


def whole_units(tokens, gate_weight, up_weight, down_weight, out_grad):
    down_full = lax.all_gather(down_weight, "fs", axis=1, tiled=True)
    gate_full = lax.all_gather(gate_weight, "fs", axis=0, tiled=True)
    up_full = lax.all_gather(up_weight, "fs", axis=0, tiled=True)
    gate_pre = jnp.dot(tokens, gate_full, preferred_element_type=F32)
    up_pre = jnp.dot(tokens, up_full, preferred_element_type=F32)
    sigma = jax.nn.sigmoid(gate_pre)
    activated = gate_pre * sigma
    hidden = (activated * up_pre).astype(BF16)
    hid_grad = contract_last(out_grad, down_full)
    up_grad = (hid_grad * activated).astype(BF16)
    gate_grad = (hid_grad * up_pre * sigma * (1.0 + gate_pre * (1.0 - sigma))).astype(BF16)
    partial_value = contract_last(gate_grad, gate_full) + contract_last(up_grad, up_full)
    input_grad = lax.psum(partial_value.astype(BF16), "tp")
    columns = lax.all_to_all(out_grad, "fs", split_axis=1, concat_axis=0, tiled=True)
    shard = contract_first(lax.all_gather(hidden, "fs", axis=0, tiled=True), columns)
    shard = lax.psum(shard.astype(BF16), "rep").astype(F32)
    norms = lax.psum(jnp.sum(shard * shard, axis=1), "fs")
    return (input_grad, shard, norms)


def solution(mesh):
    n, rep, tp = mesh.shape["fs"], mesh.shape["rep"], mesh.shape["tp"]

    def on_device(tokens, gate_weight, up_weight, down_weight, out_grad):
        width, both = gate_weight.shape
        if rep == 2 and tp == 4 and 2 <= n <= 4 and both % 32 == 0 and width % 256 == 0:
            return split_units(n, tokens, gate_weight, up_weight, down_weight, out_grad)
        return whole_units(tokens, gate_weight, up_weight, down_weight, out_grad)

    return jax.shard_map(
        on_device,
        mesh=mesh,
        in_specs=(
            P(("rep", "fs"), None),
            P("fs", "tp"),
            P("fs", "tp"),
            P("tp", "fs"),
            P(("rep", "fs"), None),
        ),
        out_specs=(P(("rep", "fs"), None), P("tp", "fs"), P("tp")),
        check_vma=False,
    )
```

profile of v0, /device:TPU:0, one launch (start us, length us, event | category | flops | bytes accessed | tf_op | source)
XLA Modules:
  0.0 112.2 jit_solution(3318918997488490144)
XLA Ops:
  0.6 2.0 %dynamic-slice_bitcast_fusion = (bf16[352,512]{1,0:T(8,128)(2,1)}, bf16[352,512]{1,0:T(8,128)(2,1)}) fusion(bf16[512,704]{0,1:T(8,128)(2,1)} %param.7, s32[]{:T(128)S(6)} %select_n.4, bf16[512,704]{0,1:T(8,128)(2,1)} %param.6), kind=kLoop, calls=%fused_computation | loop fusion | bytes 1441796 | tf_op jit(solution)/shard_map/transpose | solution.py:331
  2.6 106.5 %block.1 = (bf16[256,2048]{1,0:T(8,128)(2,1)}, bf16[704,512]{1,0:T(8,128)(2,1)}, f32[8,704]{1,0:T(8,128)}) custom-call(bf16[352,512]{1,0:T(8,128)(2,1)} %get-tuple-element.10.gate, bf16[352,512]{1,0:T(8,128)(2,1)} %get-tuple-element.9.up, bf16[704,512]{1,0:T(8,128)(2,1)} %down.1, bf16[256,2048]{1,0:T(8,128)(2,1)} %tokens.1, bf16[256,2048]{1,0:T(8,128)(2,1)} %grad.1), custom_call_target="tpu_custom_call" | custom-call | tf_op jit(solution)/shard_map/block/pallas_call | solution.py:344
  109.2 3.0 %write.1 = (bf16[256,2048]{1,0:T(8,128)(2,1)}, f32[704,512]{1,0:T(8,128)}, f32[704]{0:T(1024)}) custom-call(bf16[256,2048]{1,0:T(8,128)(2,1)} %get-tuple-element.6.flow, bf16[704,512]{1,0:T(8,128)(2,1)} %get-tuple-element.7.shard, f32[8,704]{1,0:T(8,128)} %get-tuple-element.8.rows), custom_call_target="tpu_custom_call" | custom-call | tf_op jit(solution)/shard_map/write/pallas_call | solution.py:361
where the time goes:
time: 112 us
  Pallas kernels  110 us (98%)
  local copies, waits for them, and re-layouts  2 us (2%)
    pallas_call x1, Pallas kernels, split_units(): pl.pallas_call(functools.partial(block_kernel, n), out_shape=[jax.ShapeDt...  107 us
    pallas_call x1, Pallas kernels, split_units(): pl.pallas_call(write_kernel, out_shape=[jax.ShapeDtypeStruct((rows, depth...  3.01 us

commit v1 on v0

v1 whole, which is shorter than its diff:
```python
import jax
import jax.numpy as jnp
from jax import lax
from jax.experimental import pallas as pl
from jax.experimental.pallas import tpu as pltpu
from jax.sharding import PartitionSpec as P

MESH = pl.DeviceIdType.MESH
BF16 = jnp.bfloat16
F32 = jnp.float32


def contract_last(left, right):
    return lax.dot_general(left, right, (((1,), (1,)), ((), ())), preferred_element_type=F32)


def contract_first(left, right):
    return lax.dot_general(left, right, (((0,), (0,)), ((), ())), preferred_element_type=F32)


def block_kernel(
    gate, up, down, tokens, grad, input_grad, down_grad, norms,
    gate_all, up_all, down_all, tokens_all, grad_all,
    gate_pre, up_pre, hid, gate_grad, up_grad, hid_all, hid_out,
    part, part_own, d_in, d_pass,
    f_out, f_in, g_own, g_out, g_in, h_out, h_in, whole_out, s_own, s_other, n_own, n_in,
    own_sem, w_send, w_recv, w_pass, y_send, y_recv, t_send, t_recv, hid_send, hid_recv,
    d_send, d_recv, e_send, e_recv, g_send, g_recv, s_send, s_recv, n_send, n_recv,
):
    n = 4
    f = lax.axis_index("fs")
    r = lax.axis_index("rep")
    t = lax.axis_index("tp")
    c, x = lax.rem(t, 2), t // 2
    h = lax.rem(f, 2)
    middle = (f == 1) | (f == 2)
    mate, far, pair = {"tp": x * 2 + 1 - c}, {"tp": (1 - x) * 2 + c}, {"rep": 1 - r}
    other = (f, f + 1 - 2 * h, lax.rem(f + 2, n), n - 1 - f)
    rows, depth = tokens.shape
    width = gate.shape[1]
    units, sub = gate_all.shape[0], hid_out.shape[1]
    half, quarter = depth // 2, rows // 4
    pieces = g_out.shape[0]
    size = half // pieces
    strip = width // 2
    shards = ((gate, gate_all), (up, up_all), (down, down_all))

    def cols(start, size):
        return pl.ds(pl.multiple_of(start, size), size)

    def tile(start, size):
        return pl.ds(pl.multiple_of(start, 16), size)

    def remote(src, dst, send, recv, peer):
        return pltpu.make_async_remote_copy(
            src_ref=src, dst_ref=dst, send_sem=send, recv_sem=recv,
            device_id=peer, device_id_type=MESH,
        )

    local = []
    places = [(tokens, tokens_all.at[pl.ds(0, rows)]), (grad, grad_all.at[pl.ds(0, rows)])]
    for own, whole in shards:
        for b in range(2):
            places.append((
                own.at[tile(h * units + (r if b == 0 else 1 - r) * sub, sub)],
                whole.at[pl.ds(b * sub, sub), cols(f * width, width)],
            ))
    for i, (own, place) in enumerate(places):
        copy = pltpu.make_async_copy(own, place, own_sem.at[i])
        copy.start()
        local.append(copy)

    barrier = pltpu.get_barrier_semaphore()
    peers = [{"rep": lax.rem(r + a, 2), "fs": other[k]}
             for a in range(2) for k in range(n) if a or k]
    for peer in peers + [mate, far]:
        pl.semaphore_signal(barrier, inc=1, device_id=peer, device_id_type=MESH)
    pl.semaphore_wait(barrier, 2 * n + 1)

    def slot(w, k):
        return shards[w][1].at[pl.ds(0, sub), cols(other[k] * width, width)]

    def weight(w, k):
        own, whole = shards[w]
        start = (h if k == 2 else 1 - h) * units + r * sub
        return remote(
            own.at[tile(start, sub)], whole.at[pl.ds(0, sub), cols(f * width, width)],
            w_send.at[w, k], w_recv.at[w, k], {"fs": other[k]},
        )

    def relay(w):
        return remote(slot(w, 1), slot(w, 1), w_pass.at[w], w_recv.at[w, 3], {"fs": other[2]})

    def across(w, k):
        place = cols(other[k] * width, width)
        return remote(
            shards[w][1].at[pl.ds(0, sub), place], shards[w][1].at[pl.ds(sub, sub), place],
            y_send.at[w, k], y_recv.at[w, k], pair,
        )

    def give(w, ks):
        for k in ks:
            if k == 3:
                @pl.when(middle)
                def _():
                    weight(w, k).start()
            else:
                weight(w, k).start()

    def arrive(w, k):
        weight(w, k).wait_recv()
        across(w, k).start()
        if k == 1:
            @pl.when(middle)
            def _():
                relay(w).start()

    flows = ((tokens, tokens_all, 1), (grad, grad_all, 1), (grad, grad_all, 2), (grad, grad_all, 3))

    def span(i, q):
        return flows[i][1].at[tile(flows[i][2] * rows + q * quarter, quarter)]

    q_near, q_far, q_mate, q_cross = t, (1 - x) * 2 + c, x * 2 + 1 - c, (1 - x) * 2 + 1 - c

    def fetch(i):
        own = grad_all.at[tile(rows + t * quarter, quarter)] if i == 3 else (
            flows[i][0].at[tile(t * quarter, quarter)])
        return remote(own, span(i, q_near), t_send.at[i, 0], t_recv.at[i, 0],
                      {"fs": other[1]} if i < 2 else pair)

    def spread(i, j):
        q = q_near if j < 3 else q_far
        return remote(span(i, q), span(i, q), t_send.at[i, j], t_recv.at[i, j],
                      far if j == 1 else mate)

    def hand(i):
        fetch(i).wait_recv()
        spread(i, 1).start()
        spread(i, 2).start()

    def pass_on(i):
        spread(i, 1).wait_recv()
        spread(i, 3).start()

    def complete(i):
        spread(i, 2).wait_recv()
        spread(i, 3).wait_recv()

    fetch(0).start()
    fetch(2).start()
    give(0, (1, 2, 3))
    fetch(1).start()
    give(1, (1, 2, 3))

    def pre(w, k):
        at = cols(other[k] * width, width)
        target = gate_pre if w == 0 else up_pre
        product = contract_last(tokens_all[:, at], shards[w][1][:, at])
        if k == 0:
            target[...] = product
        else:
            target[...] += product

    hand(0)
    hand(2)
    arrive(0, 1)
    pass_on(0)
    hand(1)
    fetch(3).start()
    arrive(1, 1)
    give(2, (1, 2, 3))
    pass_on(2)
    for copy in local:
        copy.wait()
    complete(0)
    for w in range(2):
        pre(w, 0)
    arrive(0, 2)
    pass_on(1)
    hand(3)
    arrive(1, 2)
    for w in range(2):
        across(w, 1).wait_recv()
        pre(w, 1)
    pass_on(3)
    arrive(0, 3)
    for w in range(2):
        across(w, 2).wait_recv()
        pre(w, 2)
    arrive(2, 1)
    arrive(1, 3)
    for w in range(2):
        across(w, 3).wait_recv()
        pre(w, 3)

    gated, raw = gate_pre[...], up_pre[...]
    sigma = jax.nn.sigmoid(gated)
    hidden = (gated * sigma * raw).astype(BF16)
    hid_out[...] = hidden[:, sub:]
    hid_swap = remote(hid_out, hid_all.at[pl.ds(2 * rows, 2 * rows)],
                      hid_send.at[0], hid_recv.at[0], pair)
    hid_swap.start()
    hid_all[pl.ds(0, 2 * rows)] = hidden[:, :sub]
    gate_pre[...] = gated * sigma
    up_pre[...] = raw * sigma * (1.0 + gated * (1.0 - sigma))

    def add_hid(k):
        at = cols(other[k] * width, width)
        product = contract_last(grad_all[pl.ds(0, 2 * rows), at], down_all[:, at])
        if k == 0:
            hid[...] = product
        else:
            hid[...] += product

    complete(1)
    add_hid(0)
    across(2, 1).wait_recv()
    add_hid(1)
    arrive(2, 2)

    def d_direct(k):
        return remote(part.at[k], d_in.at[k], d_send.at[k], d_recv.at[k], {"fs": other[k]})

    def d_first(k):
        return remote(part.at[k], d_pass.at[k], d_send.at[k], e_recv.at[k], {"fs": other[1]})

    def d_second(k):
        return remote(d_pass.at[k], d_in.at[k], e_send.at[k], d_recv.at[k], {"fs": other[5 - k]})

    complete(2)
    complete(3)
    hid_swap.wait_recv()
    for k in (2, 3, 1, 0):
        at = cols(other[k] * width, width)
        product = contract_first(hid_all[...], grad_all[:, at])
        if k == 0:
            part_own[...] = product
        else:
            part[k] = product.astype(BF16)
            if k == 1:
                d_direct(k).start()
            else:
                @pl.when(middle)
                def _():
                    d_direct(k).start()

                @pl.when(~middle)
                def _():
                    d_first(k).start()

    across(2, 2).wait_recv()
    add_hid(2)

    @pl.when(middle)
    def _():
        for k in (2, 3):
            d_first(k).wait_recv()
            d_second(k).start()

    arrive(2, 3)
    across(2, 3).wait_recv()
    add_hid(3)

    for b in (1, 0):
        at = pl.ds(b * rows, rows)
        up_grad[at] = (hid[at] * gate_pre[at]).astype(BF16)
        gate_grad[at] = (hid[at] * up_pre[at]).astype(BF16)

    def flow(b, at):
        block = pl.ds(b * rows, rows)
        return (
            jnp.dot(gate_grad[block], gate_all[:, at], preferred_element_type=F32)
            + jnp.dot(up_grad[block], up_all[:, at], preferred_element_type=F32)
        )

    def push(i, src, dst, peer):
        copy = remote(src, dst, g_send.at[i], g_recv.at[i], peer)
        copy.start()
        return copy

    neighbour = {"fs": other[1]}
    cross = {}
    for b in (1, 0):
        f_out[b] = flow(b, cols((1 - c) * half, half)).astype(BF16)
        cross[b] = push(b, f_out.at[b], f_in.at[b], mate)
    over = []
    for b in (1, 0):
        kept = flow(b, cols(c * half, half))
        cross[b].wait()
        kept = kept + f_in[b].astype(F32)
        for q in range(pieces):
            piece = kept[:, q * size:(q + 1) * size]
            if b == 1:
                g_out[q] = piece.astype(BF16)
                over.append(push(2 + q, g_out.at[q], g_in.at[q], neighbour))
            else:
                g_own[q] = piece
    sent = []
    for q in range(pieces):
        over[q].wait()
        h_out[q] = (g_own[q] + g_in[q].astype(F32)).astype(BF16)
        sent.append(push(2 + pieces + q, h_out.at[q], h_in.at[q], far))

    for k in range(1, n):
        d_direct(k).wait_recv()
    s_own[0] = (part_own[...] + d_in[2].astype(F32)).astype(BF16)
    s_own[1] = (d_in[1].astype(F32) + d_in[3].astype(F32)).astype(BF16)
    swap = remote(s_own, s_other, s_send.at[0], s_recv.at[0], pair)
    swap.start()
    sums = []
    for b in range(2):
        kept = s_own[b].astype(F32)
        down_grad[tile((h if b == 0 else 1 - h) * units + r * sub, sub)] = s_own[b]
        sums.append(lax.dot_general(
            jnp.ones((8, width), F32), kept * kept, (((1,), (1,)), ((), ())),
            precision=lax.Precision.HIGHEST, preferred_element_type=F32,
        ))
    n_own[...] = jnp.concatenate(
        [jnp.where(h == 0, sums[0], sums[1]), jnp.where(h == 0, sums[1], sums[0])], axis=1
    )
    small = []
    for i, peer in enumerate(peers):
        copy = remote(n_own, n_in.at[i], n_send.at[i], n_recv.at[i], peer)
        copy.start()
        small.append(copy)

    beside = []
    for q in range(pieces):
        sent[q].wait()
        at = cols(c * half + q * size, size)
        whole_out[:, at] = (h_out[q].astype(F32) + h_in[q].astype(F32)).astype(BF16)
        beside.append(push(2 + 2 * pieces + q, whole_out.at[:, at], whole_out.at[:, at], mate))

    for w in range(3):
        for k in (1, 2):
            weight(w, k).wait_send()

        @pl.when(middle)
        def _():
            weight(w, 3).wait_send()
            relay(w).wait_send()

        for k in range(1, n):
            across(w, k).wait_send()
    for i in range(4):
        fetch(i).wait_send()
        for j in range(1, 4):
            spread(i, j).wait_send()
    hid_swap.wait_send()
    for k in range(1, n):
        d_direct(k).wait_send()

    @pl.when(middle)
    def _():
        for k in (2, 3):
            d_second(k).wait_send()

    for copy in small:
        copy.wait()
    here = n_own[...]
    for i in range(n - 1):
        here = here + n_in[i]
    there = n_in[n - 1]
    for i in range(n, 2 * n - 1):
        there = there + n_in[i]
    first, second = jnp.where(r == 0, here, there), jnp.where(r == 0, there, here)
    norms[...] = jnp.concatenate(
        [first[:, :sub], second[:, :sub], first[:, sub:], second[:, sub:]], axis=1
    )
    swap.wait()
    for b in range(2):
        down_grad[tile((h if b == 0 else 1 - h) * units + (1 - r) * sub, sub)] = s_other[b]
    for copy in beside:
        copy.wait()
    input_grad[...] = whole_out[...]


def write_kernel(flow, shard, rows, input_grad, down_grad, norms):
    input_grad[...] = flow[...]
    down_grad[...] = shard[...].astype(F32)
    norms[...] = rows[0]


def split_units(tokens, gate_weight, up_weight, down_weight, out_grad):
    rows, depth = tokens.shape
    width, both = gate_weight.shape
    units, sub = both // 2, both // 4
    anywhere = pl.BlockSpec(memory_space=pl.ANY)
    vmem = pl.BlockSpec(memory_space=pltpu.VMEM)
    dma = pltpu.SemaphoreType.DMA
    n, half, pieces = 4, depth // 2, 4
    piece = (pieces, rows, half // pieces)
    peers = 2 * n - 1
    scratch = [((units, depth), BF16)] * 3 + [((2 * rows, depth), BF16), ((4 * rows, depth), BF16)]
    scratch += [((2 * rows, units), F32)] * 3 + [((2 * rows, units), BF16)] * 2
    scratch += [((4 * rows, sub), BF16), ((2 * rows, sub), BF16)]
    scratch += [((n, sub, width), BF16), ((sub, width), F32)] + [((n, sub, width), BF16)] * 2
    scratch += [((2, rows, half), BF16)] * 2 + [(piece, F32)] + [(piece, BF16)] * 4
    scratch += [((rows, depth), BF16)] + [((2, sub, width), BF16)] * 2
    scratch += [((8, units), F32), ((peers, 8, units), F32)]
    input_grad, down_grad, norms = pl.pallas_call(
        block_kernel,
        out_shape=[
            jax.ShapeDtypeStruct((rows, depth), BF16),
            jax.ShapeDtypeStruct((both, width), BF16),
            jax.ShapeDtypeStruct((8, both), F32),
        ],
        in_specs=[anywhere] * 5,
        out_specs=[vmem] * 3,
        scratch_shapes=[pltpu.VMEM(shape, kind) for shape, kind in scratch] + [
            dma((8,)), dma((3, n)), dma((3, n)), dma((3,)), dma((3, n)), dma((3, n)),
            dma((4, 4)), dma((4, 4)), dma((1,)), dma((1,)),
            dma((n,)), dma((n,)), dma((n,)), dma((n,)),
            dma((2 + 3 * pieces,)), dma((2 + 3 * pieces,)),
            dma((1,)), dma((1,)), dma((peers,)), dma((peers,)),
        ],
        compiler_params=pltpu.CompilerParams(collective_id=0, has_side_effects=True),
        name="block",
    )(gate_weight.T, up_weight.T, down_weight, tokens, out_grad)
    return tuple(pl.pallas_call(
        write_kernel,
        out_shape=[
            jax.ShapeDtypeStruct((rows, depth), BF16),
            jax.ShapeDtypeStruct((both, width), F32),
            jax.ShapeDtypeStruct((both,), F32),
        ],
        in_specs=[vmem] * 3,
        out_specs=[vmem] * 3,
        name="write",
    )(input_grad, down_grad, norms))


def whole_units(tokens, gate_weight, up_weight, down_weight, out_grad):
    down_full = lax.all_gather(down_weight, "fs", axis=1, tiled=True)
    gate_full = lax.all_gather(gate_weight, "fs", axis=0, tiled=True)
    up_full = lax.all_gather(up_weight, "fs", axis=0, tiled=True)
    gate_pre = jnp.dot(tokens, gate_full, preferred_element_type=F32)
    up_pre = jnp.dot(tokens, up_full, preferred_element_type=F32)
    sigma = jax.nn.sigmoid(gate_pre)
    activated = gate_pre * sigma
    hidden = (activated * up_pre).astype(BF16)
    hid_grad = contract_last(out_grad, down_full)
    up_grad = (hid_grad * activated).astype(BF16)
    gate_grad = (hid_grad * up_pre * sigma * (1.0 + gate_pre * (1.0 - sigma))).astype(BF16)
    partial_value = contract_last(gate_grad, gate_full) + contract_last(up_grad, up_full)
    input_grad = lax.psum(partial_value.astype(BF16), "tp")
    columns = lax.all_to_all(out_grad, "fs", split_axis=1, concat_axis=0, tiled=True)
    shard = contract_first(lax.all_gather(hidden, "fs", axis=0, tiled=True), columns)
    shard = lax.psum(shard.astype(BF16), "rep").astype(F32)
    norms = lax.psum(jnp.sum(shard * shard, axis=1), "fs")
    return (input_grad, shard, norms)


def solution(mesh):
    n, rep, tp = mesh.shape["fs"], mesh.shape["rep"], mesh.shape["tp"]

    def on_device(tokens, gate_weight, up_weight, down_weight, out_grad):
        width, both = gate_weight.shape
        if rep == 2 and tp == 4 and n == 4 and both % 64 == 0 and width % 256 == 0 and tokens.shape[0] % 64 == 0:
            return split_units(tokens, gate_weight, up_weight, down_weight, out_grad)
        return whole_units(tokens, gate_weight, up_weight, down_weight, out_grad)

    return jax.shard_map(
        on_device,
        mesh=mesh,
        in_specs=(
            P(("rep", "fs"), None),
            P("fs", "tp"),
            P("fs", "tp"),
            P("tp", "fs"),
            P(("rep", "fs"), None),
        ),
        out_specs=(P(("rep", "fs"), None), P("tp", "fs"), P("tp")),
        check_vma=False,
    )
```

time: 112 us -> 127 us (1.13)
  Pallas kernels: 110 us -> 126 us
  local copies, waits for them, and re-layouts: 2 us -> 0 us
    pallas_call x1, Pallas kernels: 107 us -> 123 us  [split_units(): pl.pallas_call(block_kernel, out_shape=[jax.ShapeDtypeStruct((rows, depth...]
    transpose x1 -> x0, local copies, waits for them, and re-layouts: 2 us -> none  [split_units(): up = lax.dynamic_slice_in_dim(up_weight, start, units, 1).T]
where the time goes in v1:
time: 127 us
  Pallas kernels  126 us (99%)
    pallas_call x1, Pallas kernels, split_units(): pl.pallas_call(block_kernel, out_shape=[jax.ShapeDtypeStruct((rows, depth...  123 us
    pallas_call x1, Pallas kernels, split_units(): pl.pallas_call(write_kernel, out_shape=[jax.ShapeDtypeStruct((rows, depth...  3.01 us

profile of v1, /device:TPU:0, one launch (start us, length us, event | category | flops | bytes accessed | tf_op | source)
XLA Modules:
  0.0 126.9 jit_solution(16470319372881836370)
XLA Ops:
  0.6 123.2 %block.1 = (bf16[256,2048]{1,0:T(8,128)(2,1)}, bf16[704,512]{1,0:T(8,128)(2,1)}, f32[8,704]{1,0:T(8,128)}) custom-call(bf16[704,512]{1,0:T(8,128)(2,1)} %bitcast.2, bf16[704,512]{1,0:T(8,128)(2,1)} %bitcast.3, bf16[704,512]{1,0:T(8,128)(2,1)} %down.1, bf16[256,2048]{1,0:T(8,128)(2,1)} %tokens.1, bf16[256,2048]{1,0:T(8,128)(2,1)} %grad.1), custom_call_target="tpu_custom_call" | custom-call | tf_op jit(solution)/shard_map/block/pallas_call | solution.py:401
  123.9 3.0 %write.1 = (bf16[256,2048]{1,0:T(8,128)(2,1)}, f32[704,512]{1,0:T(8,128)}, f32[704]{0:T(1024)}) custom-call(bf16[256,2048]{1,0:T(8,128)(2,1)} %get-tuple-element.6.flow, bf16[704,512]{1,0:T(8,128)(2,1)} %get-tuple-element.7.shard, f32[8,704]{1,0:T(8,128)} %get-tuple-element.8.rows), custom_call_target="tpu_custom_call" | custom-call | tf_op jit(solution)/shard_map/write/pallas_call | solution.py:420

commit v2 on v1

v2 whole, which is shorter than its diff:
```python
import jax
import jax.numpy as jnp
from jax import lax
from jax.experimental import pallas as pl
from jax.experimental.pallas import tpu as pltpu
from jax.sharding import PartitionSpec as P

MESH = pl.DeviceIdType.MESH
BF16 = jnp.bfloat16
F32 = jnp.float32


def contract_last(left, right):
    return lax.dot_general(left, right, (((1,), (1,)), ((), ())), preferred_element_type=F32)


def contract_first(left, right):
    return lax.dot_general(left, right, (((0,), (0,)), ((), ())), preferred_element_type=F32)


def block_kernel(
    gate, up, down, tokens, grad, input_grad, down_grad, norms,
    gate_all, up_all, down_all, tokens_all, grad_all,
    gate_pre, up_pre, hid, gate_grad, up_grad, hid_all, hid_out,
    part, part_own, d_in, d_pass,
    f_out, f_in, g_own, g_out, g_in, h_out, h_in, whole_out, s_own, s_other, n_own, n_in,
    own_sem, w_send, w_recv, w_pass, y_send, y_recv, t_send, t_recv, hid_send, hid_recv,
    d_send, d_recv, e_send, e_recv, g_send, g_recv, s_send, s_recv, n_send, n_recv,
):
    n = 4
    f = lax.axis_index("fs")
    r = lax.axis_index("rep")
    t = lax.axis_index("tp")
    c, x = lax.rem(t, 2), t // 2
    h = lax.rem(f, 2)
    middle = (f == 1) | (f == 2)
    mate, far, pair = {"tp": x * 2 + 1 - c}, {"tp": (1 - x) * 2 + c}, {"rep": 1 - r}
    other = (f, f + 1 - 2 * h, lax.rem(f + 2, n), n - 1 - f)
    rows, depth = tokens.shape
    width = gate.shape[1]
    units, sub = gate_all.shape[0], hid_out.shape[1]
    half, quarter = depth // 2, rows // 4
    pieces = g_out.shape[0]
    size = half // pieces
    shards = ((gate, gate_all), (up, up_all), (down, down_all))

    def cols(start, size):
        return pl.ds(pl.multiple_of(start, size), size)

    def tile(start, size):
        return pl.ds(pl.multiple_of(start, 16), size)

    def remote(src, dst, send, recv, peer):
        return pltpu.make_async_remote_copy(
            src_ref=src, dst_ref=dst, send_sem=send, recv_sem=recv,
            device_id=peer, device_id_type=MESH,
        )

    local = []
    places = [(tokens, tokens_all.at[pl.ds(0, rows)]), (grad, grad_all.at[pl.ds(0, rows)])]
    for own, whole in shards:
        for b in range(2):
            places.append((
                own.at[tile(h * units + (r if b == 0 else 1 - r) * sub, sub)],
                whole.at[pl.ds(b * sub, sub), cols(f * width, width)],
            ))
    for i, (own, place) in enumerate(places):
        copy = pltpu.make_async_copy(own, place, own_sem.at[i])
        copy.start()
        local.append(copy)

    barrier = pltpu.get_barrier_semaphore()
    peers = [{"rep": lax.rem(r + a, 2), "fs": other[k]}
             for a in range(2) for k in range(n) if a or k]
    for peer in peers + [mate, far]:
        pl.semaphore_signal(barrier, inc=1, device_id=peer, device_id_type=MESH)
    pl.semaphore_wait(barrier, 2 * n + 1)

    cuts = (1, 1, 2)

    def place(w, k, j):
        size = width // cuts[w]
        return cols(other[k] * width + j * size, size)

    def weight(w, k, j):
        own, whole = shards[w]
        start = (h if k == 2 else 1 - h) * units + r * sub
        size = width // cuts[w]
        return remote(
            own.at[tile(start, sub), pl.ds(j * size, size)],
            whole.at[pl.ds(0, sub), place(w, 0, j)],
            w_send.at[w, k, j], w_recv.at[w, k, j], {"fs": other[k]},
        )

    def relay(w, j):
        slot = shards[w][1].at[pl.ds(0, sub), place(w, 1, j)]
        return remote(slot, slot, w_pass.at[w, j], w_recv.at[w, 3, j], {"fs": other[2]})

    def across(w, k, j):
        whole = shards[w][1]
        return remote(
            whole.at[pl.ds(0, sub), place(w, k, j)], whole.at[pl.ds(sub, sub), place(w, k, j)],
            y_send.at[w, k, j], y_recv.at[w, k, j], pair,
        )

    flows = ((tokens, tokens_all, 1), (grad, grad_all, 1), (grad, grad_all, 2), (grad, grad_all, 3))

    def span(i, q):
        return flows[i][1].at[tile(flows[i][2] * rows + q * quarter, quarter)]

    q_near, q_far = t, (1 - x) * 2 + c

    def fetch(i):
        own = grad_all.at[tile(rows + t * quarter, quarter)] if i == 3 else (
            flows[i][0].at[tile(t * quarter, quarter)])
        return remote(own, span(i, q_near), t_send.at[i, 0], t_recv.at[i, 0],
                      {"fs": other[1]} if i < 2 else pair)

    def spread(i, j):
        q = q_near if j < 3 else q_far
        return remote(span(i, q), span(i, q), t_send.at[i, j], t_recv.at[i, j],
                      far if j == 1 else mate)

    def hand(i):
        fetch(i).wait_recv()
        spread(i, 1).start()
        spread(i, 2).start()

    def pass_on(i):
        spread(i, 1).wait_recv()
        spread(i, 3).start()

    def complete(i):
        spread(i, 2).wait_recv()
        spread(i, 3).wait_recv()

    def body(mid):
        def give(w, k):
            for j in range(cuts[w]):
                weight(w, k, j).start()

        def arrive(w, k):
            for j in range(cuts[w]):
                weight(w, k, j).wait_recv()
                if k == 1 and mid:
                    relay(w, j).start()
                across(w, k, j).start()

        def arrived(w, k):
            for j in range(cuts[w]):
                across(w, k, j).wait_recv()

        def pre(k):
            at = place(0, k, 0)
            for w, target in ((0, gate_pre), (1, up_pre)):
                if k:
                    arrived(w, k)
                product = contract_last(tokens_all[:, at], shards[w][1][:, at])
                if k == 0:
                    target[...] = product
                else:
                    target[...] += product

        def start_pre():
            for copy in local:
                copy.wait()
            complete(0)
            pre(0)

        hid_swap = remote(hid_out, hid_all.at[pl.ds(2 * rows, 2 * rows)],
                          hid_send.at[0], hid_recv.at[0], pair)

        def activate():
            gated, raw = gate_pre[...], up_pre[...]
            sigma = jax.nn.sigmoid(gated)
            hidden = (gated * sigma * raw).astype(BF16)
            hid_out[...] = hidden[:, sub:]
            hid_swap.start()
            hid_all[pl.ds(0, 2 * rows)] = hidden[:, :sub]
            gate_pre[...] = gated * sigma
            up_pre[...] = raw * sigma * (1.0 + gated * (1.0 - sigma))

        def add_hid(k):
            if k:
                arrived(2, k)
            else:
                complete(1)
            at = cols(other[k] * width, width)
            product = contract_last(grad_all[pl.ds(0, 2 * rows), at], down_all[:, at])
            if k == 0:
                hid[...] = product
            else:
                hid[...] += product

        def d_direct(k):
            return remote(part.at[k], d_in.at[k], d_send.at[k], d_recv.at[k], {"fs": other[k]})

        def d_first(k):
            return remote(part.at[k], d_pass.at[k], d_send.at[k], e_recv.at[k], {"fs": other[1]})

        def d_second(k):
            return remote(d_pass.at[k], d_in.at[k], e_send.at[k], d_recv.at[k], {"fs": other[5 - k]})

        def products():
            complete(2)
            complete(3)
            hid_swap.wait_recv()
            for k in (2, 3, 1, 0):
                at = cols(other[k] * width, width)
                product = contract_first(hid_all[...], grad_all[:, at])
                if k == 0:
                    part_own[...] = product
                    continue
                part[k] = product.astype(BF16)
                (d_direct if mid or k == 1 else d_first)(k).start()

        def hand_products():
            for k in (2, 3):
                d_first(k).wait_recv()
                d_second(k).start()

        def flow(b, at):
            span = pl.ds(b * rows, rows)
            return (
                jnp.dot(gate_grad[span], gate_all[:, at], preferred_element_type=F32)
                + jnp.dot(up_grad[span], up_all[:, at], preferred_element_type=F32)
            )

        def push(i, src, dst, peer):
            copy = remote(src, dst, g_send.at[i], g_recv.at[i], peer)
            copy.start()
            return copy

        def rows_done():
            for k in range(1, n):
                d_direct(k).wait_recv()
            s_own[0] = (part_own[...] + d_in[2].astype(F32)).astype(BF16)
            s_own[1] = (d_in[1].astype(F32) + d_in[3].astype(F32)).astype(BF16)
            sums = []
            for b in range(2):
                kept = s_own[b].astype(F32)
                down_grad[tile((h if b == 0 else 1 - h) * units + r * sub, sub)] = s_own[b]
                sums.append(lax.dot_general(
                    jnp.ones((8, width), F32), kept * kept, (((1,), (1,)), ((), ())),
                    precision=lax.Precision.HIGHEST, preferred_element_type=F32,
                ))
            n_own[...] = jnp.concatenate(
                [jnp.where(h == 0, sums[0], sums[1]), jnp.where(h == 0, sums[1], sums[0])], axis=1
            )
            small = []
            for i, peer in enumerate(peers):
                copy = remote(n_own, n_in.at[i], n_send.at[i], n_recv.at[i], peer)
                copy.start()
                small.append(copy)
            swap = remote(s_own, s_other, s_send.at[0], s_recv.at[0], pair)
            swap.start()
            return swap, small

        if mid:
            fetch(2).start()
            fetch(0).start()
            for k in (1, 3, 2):
                give(0, k)
            fetch(1).start()
            for k in (1, 3, 2):
                give(1, k)
            arrive(0, 1)
            arrive(0, 3)
            hand(0)
            arrive(1, 1)
            for k in (1, 3, 2):
                give(2, k)
            hand(2)
            arrive(1, 3)
            pass_on(0)
            start_pre()
            arrive(0, 2)
            pre(1)
            hand(1)
            fetch(3).start()
            pass_on(2)
            pre(3)
            arrive(1, 2)
            pass_on(1)
            hand(3)
            arrive(2, 1)
            pre(2)
            pass_on(3)
            activate()
            add_hid(0)
            add_hid(1)
            arrive(2, 3)
            arrive(2, 2)
            products()
            add_hid(3)
            add_hid(2)
        else:
            fetch(2).start()
            give(0, 1)
            fetch(0).start()
            give(1, 1)
            give(0, 2)
            fetch(1).start()
            give(1, 2)
            give(2, 1)
            give(2, 2)
            hand(2)
            arrive(0, 2)
            hand(0)
            arrive(0, 1)
            pass_on(0)
            arrive(1, 2)
            pass_on(2)
            hand(1)
            fetch(3).start()
            arrive(0, 3)
            pass_on(1)
            start_pre()
            hand(3)
            arrive(1, 1)
            arrive(1, 3)
            pre(2)
            pre(1)
            pre(3)
            activate()
            pass_on(3)
            arrive(2, 2)
            add_hid(0)
            arrive(2, 1)
            arrive(2, 3)
            products()
            add_hid(2)
            add_hid(1)
            add_hid(3)

        neighbour = {"fs": other[1]}
        cross = {}
        for b in (1, 0):
            at = pl.ds(b * rows, rows)
            up_grad[at] = (hid[at] * gate_pre[at]).astype(BF16)
            gate_grad[at] = (hid[at] * up_pre[at]).astype(BF16)
            f_out[b] = flow(b, cols((1 - c) * half, half)).astype(BF16)
            cross[b] = push(b, f_out.at[b], f_in.at[b], mate)
        over = []
        for b in (1, 0):
            kept = flow(b, cols(c * half, half))
            cross[b].wait()
            kept = kept + f_in[b].astype(F32)
            for q in range(pieces):
                piece = kept[:, q * size:(q + 1) * size]
                if b == 1:
                    g_out[q] = piece.astype(BF16)
                    over.append(push(2 + q, g_out.at[q], g_in.at[q], neighbour))
                else:
                    g_own[q] = piece
        if mid:
            hand_products()
        sent = []
        for q in range(pieces):
            over[q].wait()
            h_out[q] = (g_own[q] + g_in[q].astype(F32)).astype(BF16)
            sent.append(push(2 + pieces + q, h_out.at[q], h_in.at[q], far))
        swap, small = rows_done()
        beside = []
        for q in range(pieces):
            sent[q].wait()
            at = cols(c * half + q * size, size)
            whole_out[:, at] = (h_out[q].astype(F32) + h_in[q].astype(F32)).astype(BF16)
            beside.append(push(2 + 2 * pieces + q, whole_out.at[:, at], whole_out.at[:, at], mate))

        for w in range(3):
            for j in range(cuts[w]):
                for k in (1, 2, 3) if mid else (1, 2):
                    weight(w, k, j).wait_send()
                if mid:
                    relay(w, j).wait_send()
                for k in range(1, n):
                    across(w, k, j).wait_send()
        for i in range(4):
            fetch(i).wait_send()
            for j in range(1, 4):
                spread(i, j).wait_send()
        hid_swap.wait_send()
        for k in range(1, n):
            d_direct(k).wait_send()
        if mid:
            for k in (2, 3):
                d_second(k).wait_send()

        for copy in small:
            copy.wait()
        here = n_own[...]
        for i in range(n - 1):
            here = here + n_in[i]
        there = n_in[n - 1]
        for i in range(n, 2 * n - 1):
            there = there + n_in[i]
        first, second = jnp.where(r == 0, here, there), jnp.where(r == 0, there, here)
        norms[...] = jnp.concatenate(
            [first[:, :sub], second[:, :sub], first[:, sub:], second[:, sub:]], axis=1
        )
        swap.wait()
        for b in range(2):
            down_grad[tile((h if b == 0 else 1 - h) * units + (1 - r) * sub, sub)] = s_other[b]
        for copy in beside:
            copy.wait()
        input_grad[...] = whole_out[...]

    @pl.when(middle)
    def _():
        body(True)

    @pl.when(~middle)
    def _():
        body(False)


def write_kernel(flow, shard, rows, input_grad, down_grad, norms):
    input_grad[...] = flow[...]
    down_grad[...] = shard[...].astype(F32)
    norms[...] = rows[0]


def split_units(tokens, gate_weight, up_weight, down_weight, out_grad):
    rows, depth = tokens.shape
    width, both = gate_weight.shape
    units, sub = both // 2, both // 4
    anywhere = pl.BlockSpec(memory_space=pl.ANY)
    vmem = pl.BlockSpec(memory_space=pltpu.VMEM)
    dma = pltpu.SemaphoreType.DMA
    n, half, pieces = 4, depth // 2, 4
    piece = (pieces, rows, half // pieces)
    peers = 2 * n - 1
    scratch = [((units, depth), BF16)] * 3 + [((2 * rows, depth), BF16), ((4 * rows, depth), BF16)]
    scratch += [((2 * rows, units), F32)] * 3 + [((2 * rows, units), BF16)] * 2
    scratch += [((4 * rows, sub), BF16), ((2 * rows, sub), BF16)]
    scratch += [((n, sub, width), BF16), ((sub, width), F32)] + [((n, sub, width), BF16)] * 2
    scratch += [((2, rows, half), BF16)] * 2 + [(piece, F32)] + [(piece, BF16)] * 4
    scratch += [((rows, depth), BF16)] + [((2, sub, width), BF16)] * 2
    scratch += [((8, units), F32), ((peers, 8, units), F32)]
    input_grad, down_grad, norms = pl.pallas_call(
        block_kernel,
        out_shape=[
            jax.ShapeDtypeStruct((rows, depth), BF16),
            jax.ShapeDtypeStruct((both, width), BF16),
            jax.ShapeDtypeStruct((8, both), F32),
        ],
        in_specs=[anywhere] * 5,
        out_specs=[vmem] * 3,
        scratch_shapes=[pltpu.VMEM(shape, kind) for shape, kind in scratch] + [
            dma((8,)), dma((3, n, 2)), dma((3, n, 2)), dma((3, 2)), dma((3, n, 2)), dma((3, n, 2)),
            dma((4, 4)), dma((4, 4)), dma((1,)), dma((1,)),
            dma((n,)), dma((n,)), dma((n,)), dma((n,)),
            dma((2 + 3 * pieces,)), dma((2 + 3 * pieces,)),
            dma((1,)), dma((1,)), dma((peers,)), dma((peers,)),
        ],
        compiler_params=pltpu.CompilerParams(collective_id=0, has_side_effects=True),
        name="block",
    )(gate_weight.T, up_weight.T, down_weight, tokens, out_grad)
    return tuple(pl.pallas_call(
        write_kernel,
        out_shape=[
            jax.ShapeDtypeStruct((rows, depth), BF16),
            jax.ShapeDtypeStruct((both, width), F32),
            jax.ShapeDtypeStruct((both,), F32),
        ],
        in_specs=[vmem] * 3,
        out_specs=[vmem] * 3,
        name="write",
    )(input_grad, down_grad, norms))


def whole_units(tokens, gate_weight, up_weight, down_weight, out_grad):
    down_full = lax.all_gather(down_weight, "fs", axis=1, tiled=True)
    gate_full = lax.all_gather(gate_weight, "fs", axis=0, tiled=True)
    up_full = lax.all_gather(up_weight, "fs", axis=0, tiled=True)
    gate_pre = jnp.dot(tokens, gate_full, preferred_element_type=F32)
    up_pre = jnp.dot(tokens, up_full, preferred_element_type=F32)
    sigma = jax.nn.sigmoid(gate_pre)
    activated = gate_pre * sigma
    hidden = (activated * up_pre).astype(BF16)
    hid_grad = contract_last(out_grad, down_full)
    up_grad = (hid_grad * activated).astype(BF16)
    gate_grad = (hid_grad * up_pre * sigma * (1.0 + gate_pre * (1.0 - sigma))).astype(BF16)
    partial_value = contract_last(gate_grad, gate_full) + contract_last(up_grad, up_full)
    input_grad = lax.psum(partial_value.astype(BF16), "tp")
    columns = lax.all_to_all(out_grad, "fs", split_axis=1, concat_axis=0, tiled=True)
    shard = contract_first(lax.all_gather(hidden, "fs", axis=0, tiled=True), columns)
    shard = lax.psum(shard.astype(BF16), "rep").astype(F32)
    norms = lax.psum(jnp.sum(shard * shard, axis=1), "fs")
    return (input_grad, shard, norms)


def solution(mesh):
    n, rep, tp = mesh.shape["fs"], mesh.shape["rep"], mesh.shape["tp"]

    def on_device(tokens, gate_weight, up_weight, down_weight, out_grad):
        width, both = gate_weight.shape
        if rep == 2 and tp == 4 and n == 4 and both % 64 == 0 and width % 256 == 0 and tokens.shape[0] % 64 == 0:
            return split_units(tokens, gate_weight, up_weight, down_weight, out_grad)
        return whole_units(tokens, gate_weight, up_weight, down_weight, out_grad)

    return jax.shard_map(
        on_device,
        mesh=mesh,
        in_specs=(
            P(("rep", "fs"), None),
            P("fs", "tp"),
            P("fs", "tp"),
            P("tp", "fs"),
            P(("rep", "fs"), None),
        ),
        out_specs=(P(("rep", "fs"), None), P("tp", "fs"), P("tp")),
        check_vma=False,
    )
```

time: 127 us -> 103 us (0.81)
  Pallas kernels: 126 us -> 102 us
    pallas_call x1, Pallas kernels: 123 us -> 99.3 us  [split_units(): pl.pallas_call(block_kernel, out_shape=[jax.ShapeDtypeStruct((rows, depth...]
where the time goes in v2:
time: 103 us
  Pallas kernels  102 us (99%)
    pallas_call x1, Pallas kernels, split_units(): pl.pallas_call(block_kernel, out_shape=[jax.ShapeDtypeStruct((rows, depth...  99.3 us
    pallas_call x1, Pallas kernels, split_units(): pl.pallas_call(write_kernel, out_shape=[jax.ShapeDtypeStruct((rows, depth...  3.01 us

profile of v2, /device:TPU:0, one launch (start us, length us, event | category | flops | bytes accessed | tf_op | source)
XLA Modules:
  0.0 103.0 jit_solution(15459669849245908273)
XLA Ops:
  0.6 99.3 %block.1 = (bf16[256,2048]{1,0:T(8,128)(2,1)}, bf16[704,512]{1,0:T(8,128)(2,1)}, f32[8,704]{1,0:T(8,128)}) custom-call(bf16[704,512]{1,0:T(8,128)(2,1)} %bitcast.2, bf16[704,512]{1,0:T(8,128)(2,1)} %bitcast.3, bf16[704,512]{1,0:T(8,128)(2,1)} %down.1, bf16[256,2048]{1,0:T(8,128)(2,1)} %tokens.1, bf16[256,2048]{1,0:T(8,128)(2,1)} %grad.1), custom_call_target="tpu_custom_call" | custom-call | tf_op jit(solution)/shard_map/block/pallas_call | solution.py:441
  99.9 3.0 %write.1 = (bf16[256,2048]{1,0:T(8,128)(2,1)}, f32[704,512]{1,0:T(8,128)}, f32[704]{0:T(1024)}) custom-call(bf16[256,2048]{1,0:T(8,128)(2,1)} %get-tuple-element.6.flow, bf16[704,512]{1,0:T(8,128)(2,1)} %get-tuple-element.7.shard, f32[8,704]{1,0:T(8,128)} %get-tuple-element.8.rows), custom_call_target="tpu_custom_call" | custom-call | tf_op jit(solution)/shard_map/write/pallas_call | solution.py:460

commit v3 on v2

v3 whole, which is shorter than its diff:
```python
import jax
import jax.numpy as jnp
from jax import lax
from jax.experimental import pallas as pl
from jax.experimental.pallas import tpu as pltpu
from jax.sharding import PartitionSpec as P

MESH = pl.DeviceIdType.MESH
BF16 = jnp.bfloat16
F32 = jnp.float32


def contract_last(left, right):
    return lax.dot_general(left, right, (((1,), (1,)), ((), ())), preferred_element_type=F32)


def contract_first(left, right):
    return lax.dot_general(left, right, (((0,), (0,)), ((), ())), preferred_element_type=F32)


def block_kernel(
    gate, up, down, tokens, grad, input_grad, down_grad, norms,
    gate_m, up_m, down_m, gate_e, up_e, down_e, tokens_all, grad_all,
    gate_pre, up_pre, hid, gate_grad, up_grad, hid_all_m, hid_out_m, hid_all_e, hid_out_e,
    part_m, part_e, part_own, d_in_m, d_in_e, d_pass,
    f_out, f_in, g_own, g_out, g_in, h_out, h_in, whole_out, s_own_m, s_own_e, s_other_m, s_other_e,
    n_own, n_in,
    own_sem, w_send, w_recv, w_pass, b_send, b_recv, y_send, y_recv, t_send, t_recv, hid_send, hid_recv,
    d_send, d_recv, e_send, e_recv, g_send, g_recv, s_send, s_recv, n_send, n_recv,
):
    n = 4
    f = lax.axis_index("fs")
    r = lax.axis_index("rep")
    t = lax.axis_index("tp")
    c, x = lax.rem(t, 2), t // 2
    middle = (f == 1) | (f == 2)
    mate, far, pair = {"tp": x * 2 + 1 - c}, {"tp": (1 - x) * 2 + c}, {"rep": 1 - r}
    other = (f, f + 1 - 2 * lax.rem(f, 2), lax.rem(f + 2, n), n - 1 - f)
    rows, depth = tokens.shape
    width = gate.shape[1]
    half, quarter = depth // 2, rows // 4
    pieces = g_out.shape[0]
    size = half // pieces
    owns = (gate, up, down)
    sub_m, sub_e = hid_out_m.shape[1], hid_out_e.shape[1]
    subs = {True: sub_m, False: sub_e}
    bases = {True: 2 * sub_e, False: 0}
    wholes = {True: (gate_m, up_m, down_m), False: (gate_e, up_e, down_e)}

    def cols(start, size):
        return pl.ds(pl.multiple_of(start, size), size)

    def tile(start, size):
        return pl.ds(pl.multiple_of(start, 16), size)

    def remote(src, dst, send, recv, peer):
        return pltpu.make_async_remote_copy(
            src_ref=src, dst_ref=dst, send_sem=send, recv_sem=recv,
            device_id=peer, device_id_type=MESH,
        )

    held = [
        pltpu.make_async_copy(own, whole.at[pl.ds(0, rows)], own_sem.at[i])
        for i, (own, whole) in enumerate(((tokens, tokens_all), (grad, grad_all)))
    ]

    def own_rows(mid):
        sub = subs[mid]
        return [
            pltpu.make_async_copy(
                own.at[tile(bases[mid] + (r if b == 0 else 1 - r) * sub, sub)],
                whole.at[pl.ds(b * sub, sub), cols(f * width, width)],
                own_sem.at[2 + 2 * w + b],
            )
            for w, (own, whole) in enumerate(zip(owns, wholes[mid])) for b in range(2)
        ]

    for copy in held:
        copy.start()

    barrier = pltpu.get_barrier_semaphore()
    peers = [{"rep": lax.rem(r + a, 2), "fs": other[k]}
             for a in range(2) for k in range(n) if a or k]
    for peer in peers + [mate, far]:
        pl.semaphore_signal(barrier, inc=1, device_id=peer, device_id_type=MESH)
    pl.semaphore_wait(barrier, 2 * n + 1)

    cuts = (1, 1, 2)

    def place(w, k, j):
        size = width // cuts[w]
        return cols(other[k] * width + j * size, size)

    flows = ((tokens, tokens_all, 1), (grad, grad_all, 1), (grad, grad_all, 2), (grad, grad_all, 3))

    def span(i, q):
        return flows[i][1].at[tile(flows[i][2] * rows + q * quarter, quarter)]

    q_near, q_far = t, (1 - x) * 2 + c

    def fetch(i):
        own = grad_all.at[tile(rows + t * quarter, quarter)] if i == 3 else (
            flows[i][0].at[tile(t * quarter, quarter)])
        return remote(own, span(i, q_near), t_send.at[i, 0], t_recv.at[i, 0],
                      {"fs": other[1]} if i < 2 else pair)

    def spread(i, j):
        q = q_near if j < 3 else q_far
        return remote(span(i, q), span(i, q), t_send.at[i, j], t_recv.at[i, j],
                      far if j == 1 else mate)

    def hand(i):
        fetch(i).wait_recv()
        spread(i, 1).start()
        spread(i, 2).start()

    def pass_on(i):
        spread(i, 1).wait_recv()
        spread(i, 3).start()

    def complete(i):
        spread(i, 2).wait_recv()
        spread(i, 3).wait_recv()

    def body(mid):
        sub = subs[mid]
        units = 2 * sub
        whole = wholes[mid]
        hid_all, hid_out, part = (hid_all_m, hid_out_m, part_m) if mid else (hid_all_e, hid_out_e, part_e)
        role = (mid, not mid, not mid, mid)
        local = held + own_rows(mid)
        for copy in local[2:]:
            copy.start()

        def weight(w, k, j, out=True):
            to = role[k] if out else mid
            rows_to, size = subs[to], width // cuts[w]
            return remote(
                owns[w].at[tile(bases[to] + r * rows_to, rows_to), pl.ds(j * size, size)],
                wholes[to][w].at[pl.ds(0, rows_to), place(w, 0 if out else k, j)],
                w_send.at[w, k, j], w_recv.at[w, k, j], {"fs": other[k]},
            )

        def second(w, j):
            size = width // cuts[w]
            return remote(
                owns[w].at[tile(bases[True] + (1 - r) * sub_m, sub_m), pl.ds(j * size, size)],
                wholes[True][w].at[pl.ds(sub_m, sub_m), place(w, 1 if mid else 0, j)],
                b_send.at[w, j], b_recv.at[w, j], {"fs": other[1]},
            )

        def relay(w, j):
            slot = whole[w].at[pl.ds(0, sub), place(w, 1, j)]
            return remote(slot, slot, w_pass.at[w, j], w_recv.at[w, 2, j], {"fs": other[3]})

        def across(w, k, j):
            return remote(
                whole[w].at[pl.ds(0, sub), place(w, k, j)], whole[w].at[pl.ds(sub, sub), place(w, k, j)],
                y_send.at[w, k, j], y_recv.at[w, k, j], pair,
            )

        def give(w, k):
            for j in range(cuts[w]):
                weight(w, k, j).start()

        def give_second(w):
            for j in range(cuts[w]):
                second(w, j).start()

        def arrive(w, k):
            for j in range(cuts[w]):
                weight(w, k, j, False).wait_recv()
                (relay(w, j) if mid and k == 1 else across(w, k, j)).start()

        def arrived(w, k):
            for j in range(cuts[w]):
                if mid and k == 1:
                    second(w, j).wait_recv()
                else:
                    across(w, k, j).wait_recv()

        def pre(k):
            at = place(0, k, 0)
            for w, target in ((0, gate_pre), (1, up_pre)):
                if k:
                    arrived(w, k)
                product = contract_last(tokens_all[:, at], whole[w][pl.ds(0, units), at])
                if k == 0:
                    target[:, :units] = product
                else:
                    target[:, :units] += product

        def start_pre():
            for copy in local:
                copy.wait()
            complete(0)
            pre(0)

        hid_swap = remote(hid_out, hid_all.at[pl.ds(2 * rows, 2 * rows)],
                          hid_send.at[0], hid_recv.at[0], pair)

        def activate():
            gated, raw = gate_pre[:, :units], up_pre[:, :units]
            sigma = jax.nn.sigmoid(gated)
            hidden = (gated * sigma * raw).astype(BF16)
            hid_out[...] = hidden[:, sub:]
            hid_all[pl.ds(0, 2 * rows)] = hidden[:, :sub]
            gate_pre[:, :units] = gated * sigma
            up_pre[:, :units] = raw * sigma * (1.0 + gated * (1.0 - sigma))

        def add_hid(k):
            if k:
                arrived(2, k)
            else:
                complete(1)
            at = cols(other[k] * width, width)
            product = contract_last(grad_all[pl.ds(0, 2 * rows), at], down_rows(at))
            if k == 0:
                hid[:, :units] = product
            else:
                hid[:, :units] += product

        def down_rows(at):
            return whole[2][pl.ds(0, units), at]

        def d_in(k, of):
            return (d_in_m if of else d_in_e).at[k]

        def d_direct(k):
            return remote(part.at[k], d_in(k, mid), d_send.at[k], d_recv.at[k], {"fs": other[k]})

        def d_done(k):
            return remote(d_in(k, role[k]), d_in(k, role[k]), d_send.at[k], d_recv.at[k], {"fs": other[k]})

        def d_first(k):
            return remote(part_e.at[k], d_pass.at[k], d_send.at[k], e_recv.at[k], {"fs": other[1]})

        def d_second(k):
            return remote(d_pass.at[k], d_in(k, False), e_send.at[k], d_recv.at[k], {"fs": other[5 - k]})

        def products():
            complete(2)
            complete(3)
            hid_swap.wait_recv()
            for k in (2, 3, 1, 0):
                at = cols(other[k] * width, width)
                product = contract_first(hid_all[...], grad_all[:, at])
                if k == 0:
                    part_own[pl.ds(0, sub)] = product
                    continue
                part[k] = product.astype(BF16)
                (d_direct if mid or k == 1 else d_first)(k).start()

        def hand_products():
            for k in (2, 3):
                d_first(k).wait_recv()
                d_second(k).start()

        def flow(b, at):
            span = pl.ds(b * rows, rows)
            return (
                jnp.dot(gate_grad[span, :units], whole[0][pl.ds(0, units), at],
                        preferred_element_type=F32)
                + jnp.dot(up_grad[span, :units], whole[1][pl.ds(0, units), at],
                          preferred_element_type=F32)
            )

        def push(i, src, dst, peer):
            copy = remote(src, dst, g_send.at[i], g_recv.at[i], peer)
            copy.start()
            return copy

        def rows_done():
            for k in range(1, n):
                d_done(k).wait_recv()
            sums = {}
            mine, others = (s_own_m, s_own_e) if mid else (s_own_e, s_own_m)
            mine[...] = (part_own[pl.ds(0, sub)] + d_in(3, mid)[...].astype(F32)).astype(BF16)
            others[...] = (
                d_in(1, not mid)[...].astype(F32) + d_in(2, not mid)[...].astype(F32)
            ).astype(BF16)
            for of, own in ((True, s_own_m), (False, s_own_e)):
                kept = own[...].astype(F32)
                down_grad[tile(bases[of] + r * subs[of], subs[of])] = own[...]
                sums[of] = lax.dot_general(
                    jnp.ones((8, width), F32), kept * kept, (((1,), (1,)), ((), ())),
                    precision=lax.Precision.HIGHEST, preferred_element_type=F32,
                )
            n_own[...] = jnp.concatenate([sums[False], sums[True]], axis=1)
            small = []
            for i, peer in enumerate(peers):
                copy = remote(n_own, n_in.at[i], n_send.at[i], n_recv.at[i], peer)
                copy.start()
                small.append(copy)
            swaps = []
            for i, (own, theirs) in enumerate(((s_own_m, s_other_m), (s_own_e, s_other_e))):
                copy = remote(own, theirs, s_send.at[i], s_recv.at[i], pair)
                copy.start()
                swaps.append(copy)
            return swaps, small

        if mid:
            fetch(2).start()
            fetch(0).start()
            give(0, 3)
            give(1, 3)
            give(0, 1)
            fetch(1).start()
            give(1, 1)
            arrive(0, 1)
            give(0, 2)
            give(1, 2)
            arrive(0, 3)
            hand(0)
            arrive(1, 3)
            hand(2)
            arrive(1, 1)
            for k in (1, 3, 2):
                give(2, k)
            pass_on(0)
            arrive(0, 2)
            start_pre()
            hand(1)
            fetch(3).start()
            pass_on(2)
            pre(3)
            arrive(1, 2)
            pass_on(1)
            hand(3)
            arrive(2, 3)
            pre(2)
            pre(1)
            activate()
            hid_swap.start()
            pass_on(3)
            arrive(2, 1)
            add_hid(0)
            add_hid(3)
            arrive(2, 2)
            products()
            add_hid(1)
            add_hid(2)
        else:
            fetch(2).start()
            give(0, 1)
            fetch(0).start()
            give(1, 1)
            give(0, 3)
            fetch(1).start()
            give(1, 3)
            give_second(0)
            give(2, 1)
            give_second(1)
            give(2, 3)
            give_second(2)
            hand(2)
            hand(0)
            arrive(0, 1)
            pass_on(2)
            pass_on(0)
            arrive(0, 3)
            arrive(0, 2)
            hand(1)
            fetch(3).start()
            start_pre()
            arrive(1, 2)
            arrive(1, 3)
            pass_on(1)
            arrive(1, 1)
            hand(3)
            pre(2)
            pre(1)
            arrive(2, 1)
            pre(3)
            activate()
            hid_swap.start()
            pass_on(3)
            arrive(2, 2)
            add_hid(0)
            products()
            add_hid(1)
            add_hid(2)
            arrive(2, 3)
            add_hid(3)

        neighbour = {"fs": other[1]}
        cross = {}
        for b in (1, 0):
            at = pl.ds(b * rows, rows)
            up_grad[at, :units] = (hid[at, :units] * gate_pre[at, :units]).astype(BF16)
            gate_grad[at, :units] = (hid[at, :units] * up_pre[at, :units]).astype(BF16)
            f_out[b] = flow(b, cols((1 - c) * half, half)).astype(BF16)
            cross[b] = push(b, f_out.at[b], f_in.at[b], mate)
        if mid:
            hand_products()
        over = []
        for b in (1, 0):
            kept = flow(b, cols(c * half, half))
            cross[b].wait()
            kept = kept + f_in[b].astype(F32)
            for q in range(pieces):
                piece = kept[:, q * size:(q + 1) * size]
                if b == 1:
                    g_out[q] = piece.astype(BF16)
                    over.append(push(2 + q, g_out.at[q], g_in.at[q], neighbour))
                else:
                    g_own[q] = piece
        sent = []
        for q in range(pieces):
            over[q].wait()
            h_out[q] = (g_own[q] + g_in[q].astype(F32)).astype(BF16)
            sent.append(push(2 + pieces + q, h_out.at[q], h_in.at[q], far))
            if q == 1:
                swaps, small = rows_done()
        beside = []
        for q in range(pieces):
            sent[q].wait()
            at = cols(c * half + q * size, size)
            whole_out[:, at] = (h_out[q].astype(F32) + h_in[q].astype(F32)).astype(BF16)
            beside.append(push(2 + 2 * pieces + q, whole_out.at[:, at], whole_out.at[:, at], mate))

        for w in range(3):
            for j in range(cuts[w]):
                for k in (1, 2, 3) if mid else (1, 3):
                    weight(w, k, j).wait_send()
                if mid:
                    relay(w, j).wait_send()
                else:
                    second(w, j).wait_send()
                for k in (2, 3) if mid else (1, 2, 3):
                    across(w, k, j).wait_send()
        for i in range(4):
            fetch(i).wait_send()
            for j in range(1, 4):
                spread(i, j).wait_send()
        hid_swap.wait_send()
        for k in range(1, n):
            d_direct(k).wait_send()
        if mid:
            for k in (2, 3):
                d_second(k).wait_send()

        for copy in small:
            copy.wait()
        here = n_own[...]
        for i in range(n - 1):
            here = here + n_in[i]
        there = n_in[n - 1]
        for i in range(n, 2 * n - 1):
            there = there + n_in[i]
        first, later = jnp.where(r == 0, here, there), jnp.where(r == 0, there, here)
        norms[...] = jnp.concatenate(
            [first[:, :sub_e], later[:, :sub_e], first[:, sub_e:], later[:, sub_e:]], axis=1
        )
        for copy in swaps:
            copy.wait()
        for of, theirs in ((True, s_other_m), (False, s_other_e)):
            down_grad[tile(bases[of] + (1 - r) * subs[of], subs[of])] = theirs[...]
        for copy in beside:
            copy.wait()
        input_grad[...] = whole_out[...]

    @pl.when(middle)
    def _():
        body(True)

    @pl.when(~middle)
    def _():
        body(False)


def write_kernel(flow, shard, rows, input_grad, down_grad, norms):
    input_grad[...] = flow[...]
    down_grad[...] = shard[...].astype(F32)
    norms[...] = rows[0]


def split_units(tokens, gate_weight, up_weight, down_weight, out_grad):
    rows, depth = tokens.shape
    width, both = gate_weight.shape
    sub_e = max(both * 13 // 1024, 1) * 16
    sub_m = both // 2 - sub_e
    anywhere = pl.BlockSpec(memory_space=pl.ANY)
    vmem = pl.BlockSpec(memory_space=pltpu.VMEM)
    dma = pltpu.SemaphoreType.DMA
    n, half, pieces = 4, depth // 2, 4
    piece = (pieces, rows, half // pieces)
    peers = 2 * n - 1
    scratch = [((2 * sub_m, depth), BF16)] * 3 + [((2 * sub_e, depth), BF16)] * 3
    scratch += [((2 * rows, depth), BF16), ((4 * rows, depth), BF16)]
    scratch += [((2 * rows, 2 * sub_m), F32)] * 3 + [((2 * rows, 2 * sub_m), BF16)] * 2
    for sub in (sub_m, sub_e):
        scratch += [((4 * rows, sub), BF16), ((2 * rows, sub), BF16)]
    scratch += [((n, sub_m, width), BF16), ((n, sub_e, width), BF16), ((sub_m, width), F32)]
    scratch += [((n, sub_m, width), BF16)] + [((n, sub_e, width), BF16)] * 2
    scratch += [((2, rows, half), BF16)] * 2 + [(piece, F32)] + [(piece, BF16)] * 4
    scratch += [((rows, depth), BF16)] + [((sub_m, width), BF16), ((sub_e, width), BF16)] * 2
    scratch += [((8, both // 2), F32), ((peers, 8, both // 2), F32)]
    input_grad, down_grad, norms = pl.pallas_call(
        block_kernel,
        out_shape=[
            jax.ShapeDtypeStruct((rows, depth), BF16),
            jax.ShapeDtypeStruct((both, width), BF16),
            jax.ShapeDtypeStruct((8, both), F32),
        ],
        in_specs=[anywhere] * 5,
        out_specs=[vmem] * 3,
        scratch_shapes=[pltpu.VMEM(shape, kind) for shape, kind in scratch] + [
            dma((8,)), dma((3, n, 2)), dma((3, n, 2)), dma((3, 2)), dma((3, 2)), dma((3, 2)),
            dma((3, n, 2)), dma((3, n, 2)),
            dma((4, 4)), dma((4, 4)), dma((1,)), dma((1,)),
            dma((n,)), dma((n,)), dma((n,)), dma((n,)),
            dma((2 + 3 * pieces,)), dma((2 + 3 * pieces,)),
            dma((2,)), dma((2,)), dma((peers,)), dma((peers,)),
        ],
        compiler_params=pltpu.CompilerParams(collective_id=0, has_side_effects=True),
        name="block",
    )(gate_weight.T, up_weight.T, down_weight, tokens, out_grad)
    return tuple(pl.pallas_call(
        write_kernel,
        out_shape=[
            jax.ShapeDtypeStruct((rows, depth), BF16),
            jax.ShapeDtypeStruct((both, width), F32),
            jax.ShapeDtypeStruct((both,), F32),
        ],
        in_specs=[vmem] * 3,
        out_specs=[vmem] * 3,
        name="write",
    )(input_grad, down_grad, norms))


def whole_units(tokens, gate_weight, up_weight, down_weight, out_grad):
    down_full = lax.all_gather(down_weight, "fs", axis=1, tiled=True)
    gate_full = lax.all_gather(gate_weight, "fs", axis=0, tiled=True)
    up_full = lax.all_gather(up_weight, "fs", axis=0, tiled=True)
    gate_pre = jnp.dot(tokens, gate_full, preferred_element_type=F32)
    up_pre = jnp.dot(tokens, up_full, preferred_element_type=F32)
    sigma = jax.nn.sigmoid(gate_pre)
    activated = gate_pre * sigma
    hidden = (activated * up_pre).astype(BF16)
    hid_grad = contract_last(out_grad, down_full)
    up_grad = (hid_grad * activated).astype(BF16)
    gate_grad = (hid_grad * up_pre * sigma * (1.0 + gate_pre * (1.0 - sigma))).astype(BF16)
    partial_value = contract_last(gate_grad, gate_full) + contract_last(up_grad, up_full)
    input_grad = lax.psum(partial_value.astype(BF16), "tp")
    columns = lax.all_to_all(out_grad, "fs", split_axis=1, concat_axis=0, tiled=True)
    shard = contract_first(lax.all_gather(hidden, "fs", axis=0, tiled=True), columns)
    shard = lax.psum(shard.astype(BF16), "rep").astype(F32)
    norms = lax.psum(jnp.sum(shard * shard, axis=1), "fs")
    return (input_grad, shard, norms)


def solution(mesh):
    n, rep, tp = mesh.shape["fs"], mesh.shape["rep"], mesh.shape["tp"]

    def on_device(tokens, gate_weight, up_weight, down_weight, out_grad):
        width, both = gate_weight.shape
        if rep == 2 and tp == 4 and n == 4 and both % 32 == 0 and both >= 128 and width % 256 == 0 and tokens.shape[0] % 64 == 0:
            return split_units(tokens, gate_weight, up_weight, down_weight, out_grad)
        return whole_units(tokens, gate_weight, up_weight, down_weight, out_grad)

    return jax.shard_map(
        on_device,
        mesh=mesh,
        in_specs=(
            P(("rep", "fs"), None),
            P("fs", "tp"),
            P("fs", "tp"),
            P("tp", "fs"),
            P(("rep", "fs"), None),
        ),
        out_specs=(P(("rep", "fs"), None), P("tp", "fs"), P("tp")),
        check_vma=False,
    )
```

time: 103 us -> 96.3 us (0.935)
  Pallas kernels: 102 us -> 95.5 us
    pallas_call x1, Pallas kernels: 99.3 us -> 92.5 us  [split_units(): pl.pallas_call(block_kernel, out_shape=[jax.ShapeDtypeStruct((rows, depth...]
where the time goes in v3:
time: 96.3 us; the launch traced here: 96.2 us
  Pallas kernels  95.5 us (99%)
    pallas_call x1, Pallas kernels, split_units(): pl.pallas_call(block_kernel, out_shape=[jax.ShapeDtypeStruct((rows, depth...  92.5 us
    pallas_call x1, Pallas kernels, split_units(): pl.pallas_call(write_kernel, out_shape=[jax.ShapeDtypeStruct((rows, depth...  3.01 us

profile of v3, /device:TPU:0, one launch (start us, length us, event | category | flops | bytes accessed | tf_op | source)
XLA Modules:
  0.0 96.2 jit_solution(9953881155517159352)
XLA Ops:
  0.6 92.5 %block.1 = (bf16[256,2048]{1,0:T(8,128)(2,1)}, bf16[704,512]{1,0:T(8,128)(2,1)}, f32[8,704]{1,0:T(8,128)}) custom-call(bf16[704,512]{1,0:T(8,128)(2,1)} %bitcast.2, bf16[704,512]{1,0:T(8,128)(2,1)} %bitcast.3, bf16[704,512]{1,0:T(8,128)(2,1)} %down.1, bf16[256,2048]{1,0:T(8,128)(2,1)} %tokens.1, bf16[256,2048]{1,0:T(8,128)(2,1)} %grad.1), custom_call_target="tpu_custom_call" | custom-call | tf_op jit(solution)/shard_map/block/pallas_call | solution.py:499
  93.2 3.0 %write.1 = (bf16[256,2048]{1,0:T(8,128)(2,1)}, f32[704,512]{1,0:T(8,128)}, f32[704]{0:T(1024)}) custom-call(bf16[256,2048]{1,0:T(8,128)(2,1)} %get-tuple-element.6.flow, bf16[704,512]{1,0:T(8,128)(2,1)} %get-tuple-element.7.shard, f32[8,704]{1,0:T(8,128)} %get-tuple-element.8.rows), custom_call_target="tpu_custom_call" | custom-call | tf_op jit(solution)/shard_map/write/pallas_call | solution.py:519

commit v4 on v3

--- a/solution.py
+++ b/solution.py
@@ -24,9 +24,9 @@
     gate_pre, up_pre, hid, gate_grad, up_grad, hid_all_m, hid_out_m, hid_all_e, hid_out_e,
     part_m, part_e, part_own, d_in_m, d_in_e, d_pass,
     f_out, f_in, g_own, g_out, g_in, h_out, h_in, whole_out, s_own_m, s_own_e, s_other_m, s_other_e,
-    n_own, n_in,
+    n_own, n_in, n_sum,
     own_sem, w_send, w_recv, w_pass, b_send, b_recv, y_send, y_recv, t_send, t_recv, hid_send, hid_recv,
-    d_send, d_recv, e_send, e_recv, g_send, g_recv, s_send, s_recv, n_send, n_recv,
+    d_send, d_recv, e_send, e_recv, g_send, g_recv, s_send, s_recv, n_send, n_recv, out_sem,
 ):
     n = 4
     f = lax.axis_index("fs")
@@ -70,7 +70,7 @@
             pltpu.make_async_copy(
                 own.at[tile(bases[mid] + (r if b == 0 else 1 - r) * sub, sub)],
                 whole.at[pl.ds(b * sub, sub), cols(f * width, width)],
-                own_sem.at[2 + 2 * w + b],
+                own_sem.at[2 + w],
             )
             for w, (own, whole) in enumerate(zip(owns, wholes[mid])) for b in range(2)
         ]
@@ -85,11 +85,14 @@
         pl.semaphore_signal(barrier, inc=1, device_id=peer, device_id_type=MESH)
     pl.semaphore_wait(barrier, 2 * n + 1)
 
-    cuts = (1, 1, 2)
+    cuts = (1, 1, 4)
+
+    def slot(w, k, j):
+        return w * 3 + (k - 1) * cuts[w] + j
 
     def place(w, k, j):
-        size = width // cuts[w]
-        return cols(other[k] * width + j * size, size)
+        size = width if j is None else width // cuts[w]
+        return cols(other[k] * width + (0 if j is None else j * size), size)
 
     flows = ((tokens, tokens_all, 1), (grad, grad_all, 1), (grad, grad_all, 2), (grad, grad_all, 3))
 
@@ -101,12 +104,12 @@
     def fetch(i):
         own = grad_all.at[tile(rows + t * quarter, quarter)] if i == 3 else (
             flows[i][0].at[tile(t * quarter, quarter)])
-        return remote(own, span(i, q_near), t_send.at[i, 0], t_recv.at[i, 0],
+        return remote(own, span(i, q_near), t_send.at[0], t_recv.at[i],
                       {"fs": other[1]} if i < 2 else pair)
 
     def spread(i, j):
         q = q_near if j < 3 else q_far
-        return remote(span(i, q), span(i, q), t_send.at[i, j], t_recv.at[i, j],
+        return remote(span(i, q), span(i, q), t_send.at[0], t_recv.at[(4 if j == 1 else 8) + i],
                       far if j == 1 else mate)
 
     def hand(i):
@@ -119,8 +122,8 @@
         spread(i, 3).start()
 
     def complete(i):
-        spread(i, 2).wait_recv()
-        spread(i, 3).wait_recv()
+        both_quarters = flows[i][1].at[pl.ds(0, 2 * quarter)]
+        remote(both_quarters, both_quarters, t_send.at[0], t_recv.at[8 + i], mate).wait_recv()
 
     def body(mid):
         sub = subs[mid]
@@ -128,35 +131,36 @@
         whole = wholes[mid]
         hid_all, hid_out, part = (hid_all_m, hid_out_m, part_m) if mid else (hid_all_e, hid_out_e, part_e)
         role = (mid, not mid, not mid, mid)
-        local = held + own_rows(mid)
-        for copy in local[2:]:
+        for copy in own_rows(mid):
             copy.start()
+
+        def strip(w, j):
+            size = width // cuts[w]
+            return pl.ds(0, width) if j is None else pl.ds(j * size, size)
 
         def weight(w, k, j, out=True):
             to = role[k] if out else mid
-            rows_to, size = subs[to], width // cuts[w]
             return remote(
-                owns[w].at[tile(bases[to] + r * rows_to, rows_to), pl.ds(j * size, size)],
-                wholes[to][w].at[pl.ds(0, rows_to), place(w, 0 if out else k, j)],
-                w_send.at[w, k, j], w_recv.at[w, k, j], {"fs": other[k]},
+                owns[w].at[tile(bases[to] + r * subs[to], subs[to]), strip(w, j)],
+                wholes[to][w].at[pl.ds(0, subs[to]), place(w, 0 if out else k, j)],
+                w_send.at[3 * w + k - 1], w_recv.at[slot(w, k, j or 0)], {"fs": other[k]},
             )
 
         def second(w, j):
-            size = width // cuts[w]
             return remote(
-                owns[w].at[tile(bases[True] + (1 - r) * sub_m, sub_m), pl.ds(j * size, size)],
+                owns[w].at[tile(bases[True] + (1 - r) * sub_m, sub_m), strip(w, j)],
                 wholes[True][w].at[pl.ds(sub_m, sub_m), place(w, 1 if mid else 0, j)],
-                b_send.at[w, j], b_recv.at[w, j], {"fs": other[1]},
+                b_send.at[w], b_recv.at[w], {"fs": other[1]},
             )
 
         def relay(w, j):
-            slot = whole[w].at[pl.ds(0, sub), place(w, 1, j)]
-            return remote(slot, slot, w_pass.at[w, j], w_recv.at[w, 2, j], {"fs": other[3]})
+            held_rows = whole[w].at[pl.ds(0, sub), place(w, 1, j)]
+            return remote(held_rows, held_rows, w_pass.at[w], w_recv.at[slot(w, 2, j or 0)], {"fs": other[3]})
 
         def across(w, k, j):
             return remote(
                 whole[w].at[pl.ds(0, sub), place(w, k, j)], whole[w].at[pl.ds(sub, sub), place(w, k, j)],
-                y_send.at[w, k, j], y_recv.at[w, k, j], pair,
+                y_send.at[3 * w + k - 1], y_recv.at[3 * w + k - 1], pair,
             )
 
         def give(w, k):
@@ -173,11 +177,10 @@
                 (relay(w, j) if mid and k == 1 else across(w, k, j)).start()
 
         def arrived(w, k):
-            for j in range(cuts[w]):
-                if mid and k == 1:
-                    second(w, j).wait_recv()
-                else:
-                    across(w, k, j).wait_recv()
+            if mid and k == 1:
+                second(w, None).wait_recv()
+            else:
+                across(w, k, None).wait_recv()
 
         def pre(k):
             at = place(0, k, 0)
@@ -191,8 +194,11 @@
                     target[:, :units] += product
 
         def start_pre():
-            for copy in local:
+            for copy in held:
                 copy.wait()
+            for w in range(3):
+                mine = whole[w].at[pl.ds(0, units), place(w, 0, None)]
+                pltpu.make_async_copy(mine, mine, own_sem.at[2 + w]).wait()
             complete(0)
             pre(0)
 
@@ -227,16 +233,16 @@
             return (d_in_m if of else d_in_e).at[k]
 
         def d_direct(k):
-            return remote(part.at[k], d_in(k, mid), d_send.at[k], d_recv.at[k], {"fs": other[k]})
+            return remote(part.at[k], d_in(k, mid), d_send.at[0], d_recv.at[k - 1], {"fs": other[k]})
 
         def d_done(k):
-            return remote(d_in(k, role[k]), d_in(k, role[k]), d_send.at[k], d_recv.at[k], {"fs": other[k]})
+            return remote(d_in(k, role[k]), d_in(k, role[k]), d_send.at[0], d_recv.at[k - 1], {"fs": other[k]})
 
         def d_first(k):
-            return remote(part_e.at[k], d_pass.at[k], d_send.at[k], e_recv.at[k], {"fs": other[1]})
+            return remote(part_e.at[k], d_pass.at[k], d_send.at[0], e_recv.at[k - 2], {"fs": other[1]})
 
         def d_second(k):
-            return remote(d_pass.at[k], d_in(k, False), e_send.at[k], d_recv.at[k], {"fs": other[5 - k]})
+            return remote(d_pass.at[k], d_in(k, False), e_send.at[0], d_recv.at[k - 1], {"fs": other[5 - k]})
 
         def products():
             complete(2)
@@ -265,39 +271,60 @@
                           preferred_element_type=F32)
             )
 
-        def push(i, src, dst, peer):
-            copy = remote(src, dst, g_send.at[i], g_recv.at[i], peer)
+        def push(group, i, src, dst, peer):
+            copy = remote(src, dst, g_send.at[group], g_recv.at[i], peer)
             copy.start()
             return copy
 
+        def put(group, src, dst):
+            pltpu.make_async_copy(src, dst, out_sem.at[group]).start()
+
+        swaps = [
+            remote(own, theirs, s_send.at[i], s_recv.at[i], pair)
+            for i, (own, theirs) in enumerate(((s_own_m, s_other_m), (s_own_e, s_other_e)))
+        ]
+        sums = {}
+
+        def rows_of(of):
+            own = s_own_m if of else s_own_e
+            if of == mid:
+                d_done(3).wait_recv()
+                own[...] = (part_own[pl.ds(0, sub)] + d_in(3, mid)[...].astype(F32)).astype(BF16)
+            else:
+                d_done(1).wait_recv()
+                d_done(2).wait_recv()
+                own[...] = (d_in(1, of)[...].astype(F32) + d_in(2, of)[...].astype(F32)).astype(BF16)
+            kept = own[...].astype(F32)
+            put(1, own, down_grad.at[tile(bases[of] + r * subs[of], subs[of])])
+            sums[of] = lax.dot_general(
+                jnp.ones((8, width), F32), kept * kept, (((1,), (1,)), ((), ())),
+                precision=lax.Precision.HIGHEST, preferred_element_type=F32,
+            )
+
         def rows_done():
-            for k in range(1, n):
-                d_done(k).wait_recv()
-            sums = {}
-            mine, others = (s_own_m, s_own_e) if mid else (s_own_e, s_own_m)
-            mine[...] = (part_own[pl.ds(0, sub)] + d_in(3, mid)[...].astype(F32)).astype(BF16)
-            others[...] = (
-                d_in(1, not mid)[...].astype(F32) + d_in(2, not mid)[...].astype(F32)
-            ).astype(BF16)
-            for of, own in ((True, s_own_m), (False, s_own_e)):
-                kept = own[...].astype(F32)
-                down_grad[tile(bases[of] + r * subs[of], subs[of])] = own[...]
-                sums[of] = lax.dot_general(
-                    jnp.ones((8, width), F32), kept * kept, (((1,), (1,)), ((), ())),
-                    precision=lax.Precision.HIGHEST, preferred_element_type=F32,
-                )
+            rows_of(False)
             n_own[...] = jnp.concatenate([sums[False], sums[True]], axis=1)
-            small = []
             for i, peer in enumerate(peers):
-                copy = remote(n_own, n_in.at[i], n_send.at[i], n_recv.at[i], peer)
-                copy.start()
-                small.append(copy)
-            swaps = []
-            for i, (own, theirs) in enumerate(((s_own_m, s_other_m), (s_own_e, s_other_e))):
-                copy = remote(own, theirs, s_send.at[i], s_recv.at[i], pair)
-                copy.start()
-                swaps.append(copy)
-            return swaps, small
+                remote(n_own, n_in.at[i], n_send.at[0], n_recv.at[0], peer).start()
+            swaps[1].start()
+
+        def finish_rows():
+            remote(n_in, n_in, n_send.at[0], n_recv.at[0], pair).wait_recv()
+            here = n_own[...]
+            for i in range(n - 1):
+                here = here + n_in[i]
+            there = n_in[n - 1]
+            for i in range(n, 2 * n - 1):
+                there = there + n_in[i]
+            first, later = jnp.where(r == 0, here, there), jnp.where(r == 0, there, here)
+            n_sum[...] = jnp.concatenate(
+                [first[:, :sub_e], later[:, :sub_e], first[:, sub_e:], later[:, sub_e:]], axis=1
+            )
+            put(2, n_sum, norms)
+            for copy in swaps:
+                copy.wait_recv()
+            for of, theirs in ((True, s_other_m), (False, s_other_e)):
+                put(1, theirs, down_grad.at[tile(bases[of] + (1 - r) * subs[of], subs[of])])
 
         if mid:
             fetch(2).start()
@@ -309,12 +336,12 @@
             give(1, 1)
             arrive(0, 1)
             give(0, 2)
-            give(1, 2)
             arrive(0, 3)
             hand(0)
             arrive(1, 3)
             hand(2)
             arrive(1, 1)
+            give(1, 2)
             for k in (1, 3, 2):
                 give(2, k)
             pass_on(0)
@@ -345,12 +372,12 @@
             give(0, 1)
             fetch(0).start()
             give(1, 1)
+            fetch(1).start()
             give(0, 3)
-            fetch(1).start()
             give(1, 3)
             give_second(0)
+            give_second(1)
             give(2, 1)
-            give_second(1)
             give(2, 3)
             give_second(2)
             hand(2)
@@ -358,29 +385,29 @@
             arrive(0, 1)
             pass_on(2)
             pass_on(0)
+            hand(1)
+            fetch(3).start()
             arrive(0, 3)
             arrive(0, 2)
-            hand(1)
-            fetch(3).start()
+            arrive(1, 1)
+            arrive(1, 3)
+            pass_on(1)
             start_pre()
             arrive(1, 2)
-            arrive(1, 3)
-            pass_on(1)
-            arrive(1, 1)
             hand(3)
+            pre(1)
+            pre(3)
+            pass_on(3)
+            arrive(2, 1)
             pre(2)
-            pre(1)
-            arrive(2, 1)
-            pre(3)
             activate()
             hid_swap.start()
-            pass_on(3)
             arrive(2, 2)
             add_hid(0)
+            add_hid(1)
+            arrive(2, 3)
             products()
-            add_hid(1)
             add_hid(2)
-            arrive(2, 3)
             add_hid(3)
 
         neighbour = {"fs": other[1]}
@@ -390,75 +417,67 @@
             up_grad[at, :units] = (hid[at, :units] * gate_pre[at, :units]).astype(BF16)
             gate_grad[at, :units] = (hid[at, :units] * up_pre[at, :units]).astype(BF16)
             f_out[b] = flow(b, cols((1 - c) * half, half)).astype(BF16)
-            cross[b] = push(b, f_out.at[b], f_in.at[b], mate)
-        if mid:
-            hand_products()
+            cross[b] = push(0, b, f_out.at[b], f_in.at[b], mate)
         over = []
         for b in (1, 0):
             kept = flow(b, cols(c * half, half))
-            cross[b].wait()
+            cross[b].wait_recv()
             kept = kept + f_in[b].astype(F32)
             for q in range(pieces):
                 piece = kept[:, q * size:(q + 1) * size]
                 if b == 1:
                     g_out[q] = piece.astype(BF16)
-                    over.append(push(2 + q, g_out.at[q], g_in.at[q], neighbour))
+                    over.append(push(1, 2 + q, g_out.at[q], g_in.at[q], neighbour))
                 else:
                     g_own[q] = piece
+            if b == 1 and mid:
+                hand_products()
+        rows_of(True)
+        swaps[0].start()
         sent = []
         for q in range(pieces):
-            over[q].wait()
+            over[q].wait_recv()
             h_out[q] = (g_own[q] + g_in[q].astype(F32)).astype(BF16)
-            sent.append(push(2 + pieces + q, h_out.at[q], h_in.at[q], far))
+            sent.append(push(2, 2 + pieces + q, h_out.at[q], h_in.at[q], far))
             if q == 1:
-                swaps, small = rows_done()
+                rows_done()
         beside = []
         for q in range(pieces):
-            sent[q].wait()
+            sent[q].wait_recv()
             at = cols(c * half + q * size, size)
             whole_out[:, at] = (h_out[q].astype(F32) + h_in[q].astype(F32)).astype(BF16)
-            beside.append(push(2 + 2 * pieces + q, whole_out.at[:, at], whole_out.at[:, at], mate))
+            beside.append(push(3, 2 + 2 * pieces + q, whole_out.at[:, at], whole_out.at[:, at], mate))
+            put(0, whole_out.at[:, at], input_grad.at[:, at])
+            if q == pieces - 2:
+                finish_rows()
 
         for w in range(3):
-            for j in range(cuts[w]):
-                for k in (1, 2, 3) if mid else (1, 3):
-                    weight(w, k, j).wait_send()
-                if mid:
-                    relay(w, j).wait_send()
-                else:
-                    second(w, j).wait_send()
-                for k in (2, 3) if mid else (1, 2, 3):
-                    across(w, k, j).wait_send()
-        for i in range(4):
-            fetch(i).wait_send()
-            for j in range(1, 4):
-                spread(i, j).wait_send()
+            for k in (1, 2, 3) if mid else (1, 3):
+                weight(w, k, None).wait_send()
+            (relay if mid else second)(w, None).wait_send()
+            for k in (2, 3) if mid else (1, 2, 3):
+                across(w, k, None).wait_send()
+
+        def sent_all(ref, sem):
+            remote(ref, ref, sem, sem, pair).wait_send()
+
+        sent_all(grad_all, t_send.at[0])
         hid_swap.wait_send()
-        for k in range(1, n):
-            d_direct(k).wait_send()
+        sent_all(part.at[pl.ds(1, 3)], d_send.at[0])
         if mid:
-            for k in (2, 3):
-                d_second(k).wait_send()
-
-        for copy in small:
-            copy.wait()
-        here = n_own[...]
-        for i in range(n - 1):
-            here = here + n_in[i]
-        there = n_in[n - 1]
-        for i in range(n, 2 * n - 1):
-            there = there + n_in[i]
-        first, later = jnp.where(r == 0, here, there), jnp.where(r == 0, there, here)
-        norms[...] = jnp.concatenate(
-            [first[:, :sub_e], later[:, :sub_e], first[:, sub_e:], later[:, sub_e:]], axis=1
-        )
+            sent_all(d_pass.at[pl.ds(2, 2)], e_send.at[0])
+        for i, ref in enumerate((f_out, g_out, h_out, whole_out.at[:, pl.ds(0, half)])):
+            sent_all(ref, g_send.at[i])
+        sent_all(n_in, n_send.at[0])
         for copy in swaps:
-            copy.wait()
-        for of, theirs in ((True, s_other_m), (False, s_other_e)):
-            down_grad[tile(bases[of] + (1 - r) * subs[of], subs[of])] = theirs[...]
-        for copy in beside:
-            copy.wait()
-        input_grad[...] = whole_out[...]
+            copy.wait_send()
+
+        for q in range(pieces):
+            beside[q].wait_recv()
+            at = cols((1 - c) * half + q * size, size)
+            put(0, whole_out.at[:, at], input_grad.at[:, at])
+        for i, (src, dst) in enumerate(((whole_out, input_grad), (down_grad, down_grad), (n_sum, norms))):
+            pltpu.make_async_copy(src, dst, out_sem.at[i]).wait()
 
     @pl.when(middle)
     def _():
@@ -495,7 +514,7 @@
     scratch += [((n, sub_m, width), BF16)] + [((n, sub_e, width), BF16)] * 2
     scratch += [((2, rows, half), BF16)] * 2 + [(piece, F32)] + [(piece, BF16)] * 4
     scratch += [((rows, depth), BF16)] + [((sub_m, width), BF16), ((sub_e, width), BF16)] * 2
-    scratch += [((8, both // 2), F32), ((peers, 8, both // 2), F32)]
+    scratch += [((8, both // 2), F32), ((peers, 8, both // 2), F32), ((8, both), F32)]
     input_grad, down_grad, norms = pl.pallas_call(
         block_kernel,
         out_shape=[
@@ -504,14 +523,11 @@
             jax.ShapeDtypeStruct((8, both), F32),
         ],
         in_specs=[anywhere] * 5,
-        out_specs=[vmem] * 3,
+        out_specs=[anywhere] * 3,
         scratch_shapes=[pltpu.VMEM(shape, kind) for shape, kind in scratch] + [
-            dma((8,)), dma((3, n, 2)), dma((3, n, 2)), dma((3, 2)), dma((3, 2)), dma((3, 2)),
-            dma((3, n, 2)), dma((3, n, 2)),
-            dma((4, 4)), dma((4, 4)), dma((1,)), dma((1,)),
-            dma((n,)), dma((n,)), dma((n,)), dma((n,)),
-            dma((2 + 3 * pieces,)), dma((2 + 3 * pieces,)),
-            dma((2,)), dma((2,)), dma((peers,)), dma((peers,)),
+            dma((count,)) for count in (
+                5, 9, 18, 3, 3, 3, 9, 9, 1, 12, 1, 1, 1, 3, 1, 2, 4, 2 + 3 * pieces, 2, 2, 1, 1, 3,
+            )
         ],
         compiler_params=pltpu.CompilerParams(collective_id=0, has_side_effects=True),
         name="block",
@@ -555,7 +571,7 @@
 
     def on_device(tokens, gate_weight, up_weight, down_weight, out_grad):
         width, both = gate_weight.shape
-        if rep == 2 and tp == 4 and n == 4 and both % 32 == 0 and both >= 128 and width % 256 == 0 and tokens.shape[0] % 64 == 0:
+        if rep == 2 and tp == 4 and n == 4 and both % 32 == 0 and both >= 128 and width % 512 == 0 and tokens.shape[0] % 64 == 0:
             return split_units(tokens, gate_weight, up_weight, down_weight, out_grad)
         return whole_units(tokens, gate_weight, up_weight, down_weight, out_grad)
 

time: 96.3 us -> 91 us (0.945)
  Pallas kernels: 95.5 us -> 90.2 us
    pallas_call x1, Pallas kernels: 92.5 us -> 87.2 us  [split_units(): pl.pallas_call(block_kernel, out_shape=[jax.ShapeDtypeStruct((rows, depth...]
where the time goes in v4:
time: 91 us; the launch traced here: 90.9 us
  Pallas kernels  90.2 us (99%)
    pallas_call x1, Pallas kernels, split_units(): pl.pallas_call(block_kernel, out_shape=[jax.ShapeDtypeStruct((rows, depth...  87.2 us
    pallas_call x1, Pallas kernels, split_units(): pl.pallas_call(write_kernel, out_shape=[jax.ShapeDtypeStruct((rows, depth...  3.01 us

profile of v4, /device:TPU:0, one launch (start us, length us, event | category | flops | bytes accessed | tf_op | source)
XLA Modules:
  0.0 90.9 jit_solution(9141182919658729192)
XLA Ops:
  0.6 87.2 %block.1 = (bf16[256,2048]{1,0:T(8,128)(2,1)}, bf16[704,512]{1,0:T(8,128)(2,1)}, f32[8,704]{1,0:T(8,128)}) custom-call(bf16[704,512]{1,0:T(8,128)(2,1)} %bitcast.2, bf16[704,512]{1,0:T(8,128)(2,1)} %bitcast.3, bf16[704,512]{1,0:T(8,128)(2,1)} %down.1, bf16[256,2048]{1,0:T(8,128)(2,1)} %tokens.1, bf16[256,2048]{1,0:T(8,128)(2,1)} %grad.1), custom_call_target="tpu_custom_call" | custom-call | tf_op jit(solution)/shard_map/block/pallas_call | solution.py:518
  87.9 3.0 %write.1 = (bf16[256,2048]{1,0:T(8,128)(2,1)}, f32[704,512]{1,0:T(8,128)}, f32[704]{0:T(1024)}) custom-call(bf16[256,2048]{1,0:T(8,128)(2,1)} %get-tuple-element.6.flow, bf16[704,512]{1,0:T(8,128)(2,1)} %get-tuple-element.7.shard, f32[8,704]{1,0:T(8,128)} %get-tuple-element.8.rows), custom_call_target="tpu_custom_call" | custom-call | tf_op jit(solution)/shard_map/write/pallas_call | solution.py:535

commit v5 on v4

--- a/solution.py
+++ b/solution.py
@@ -23,7 +23,7 @@
     gate_m, up_m, down_m, gate_e, up_e, down_e, tokens_all, grad_all,
     gate_pre, up_pre, hid, gate_grad, up_grad, hid_all_m, hid_out_m, hid_all_e, hid_out_e,
     part_m, part_e, part_own, d_in_m, d_in_e, d_pass,
-    f_out, f_in, g_own, g_out, g_in, h_out, h_in, whole_out, s_own_m, s_own_e, s_other_m, s_other_e,
+    f_out, f_in, g_own, g_out, g_in, x_out, x_in, h_out, h_in, whole_out, s_own_m, s_own_e, s_other_m, s_other_e,
     n_own, n_in, n_sum,
     own_sem, w_send, w_recv, w_pass, b_send, b_recv, y_send, y_recv, t_send, t_recv, hid_send, hid_recv,
     d_send, d_recv, e_send, e_recv, g_send, g_recv, s_send, s_recv, n_send, n_recv, out_sem,
@@ -39,8 +39,7 @@
     rows, depth = tokens.shape
     width = gate.shape[1]
     half, quarter = depth // 2, rows // 4
-    pieces = g_out.shape[0]
-    size = half // pieces
+    size = g_out.shape[2]
     owns = (gate, up, down)
     sub_m, sub_e = hid_out_m.shape[1], hid_out_e.shape[1]
     subs = {True: sub_m, False: sub_e}
@@ -248,7 +247,7 @@
             complete(2)
             complete(3)
             hid_swap.wait_recv()
-            for k in (2, 3, 1, 0):
+            for k in (2, 3, 1, 0) if mid else (3, 2, 1, 0):
                 at = cols(other[k] * width, width)
                 product = contract_first(hid_all[...], grad_all[:, at])
                 if k == 0:
@@ -258,7 +257,7 @@
                 (d_direct if mid or k == 1 else d_first)(k).start()
 
         def hand_products():
-            for k in (2, 3):
+            for k in (3, 2):
                 d_first(k).wait_recv()
                 d_second(k).start()
 
@@ -418,38 +417,64 @@
             gate_grad[at, :units] = (hid[at, :units] * up_pre[at, :units]).astype(BF16)
             f_out[b] = flow(b, cols((1 - c) * half, half)).astype(BF16)
             cross[b] = push(0, b, f_out.at[b], f_in.at[b], mate)
-        over = []
+        mine, theirs = 2 + x, 3 - x
+
+        def lanes(q, core=c):
+            return cols(core * half + q * size, size)
+
+        def piece(b, q):
+            return flow(b, lanes(q)) + f_in[b, :, cols(q * size, size)].astype(F32)
+
+        reduced, over = {}, []
         for b in (1, 0):
-            kept = flow(b, cols(c * half, half))
+            first = flow(b, lanes(theirs))
             cross[b].wait_recv()
-            kept = kept + f_in[b].astype(F32)
-            for q in range(pieces):
-                piece = kept[:, q * size:(q + 1) * size]
+            x_out[b] = (first + f_in[b, :, cols(theirs * size, size)].astype(F32)).astype(BF16)
+            reduced[b] = push(2, 5 + b, x_out.at[b], x_in.at[b], far)
+            for q in range(2):
                 if b == 1:
-                    g_out[q] = piece.astype(BF16)
+                    g_out[q] = piece(b, q).astype(BF16)
                     over.append(push(1, 2 + q, g_out.at[q], g_in.at[q], neighbour))
                 else:
-                    g_own[q] = piece
-            if b == 1 and mid:
-                hand_products()
-        rows_of(True)
-        swaps[0].start()
+                    g_own[q] = piece(b, q)
+            g_own[2 + b] = piece(b, mine)
+        reduced[1].wait_recv()
+        g_out[2] = (g_own[3] + x_in[1].astype(F32)).astype(BF16)
+        over.append(push(1, 4, g_out.at[2], g_in.at[2], neighbour))
+        if mid:
+            hand_products()
+        reduced[0].wait_recv()
+        g_own[2] += x_in[0].astype(F32)
         sent = []
-        for q in range(pieces):
+        for q in range(2):
             over[q].wait_recv()
             h_out[q] = (g_own[q] + g_in[q].astype(F32)).astype(BF16)
-            sent.append(push(2, 2 + pieces + q, h_out.at[q], h_in.at[q], far))
-            if q == 1:
-                rows_done()
-        beside = []
-        for q in range(pieces):
+            sent.append(push(3, 7 + q, h_out.at[q], h_in.at[q], far))
+            if q == 0:
+                rows_of(True)
+                swaps[0].start()
+        if not mid:
+            rows_done()
+        beside = {}
+
+        def finish(i, q):
+            part_out = whole_out.at[:, lanes(q)]
+            beside[i] = push(4, 10 + i, part_out, part_out, mate)
+            put(0, part_out, input_grad.at[:, lanes(q)])
+
+        over[2].wait_recv()
+        whole_out[:, lanes(mine)] = (g_own[2] + g_in[2].astype(F32)).astype(BF16)
+        gathered = push(5, 9, whole_out.at[:, lanes(mine)], whole_out.at[:, lanes(mine)], far)
+        finish(2, mine)
+        if mid:
+            rows_done()
+        for q in range(2):
             sent[q].wait_recv()
-            at = cols(c * half + q * size, size)
-            whole_out[:, at] = (h_out[q].astype(F32) + h_in[q].astype(F32)).astype(BF16)
-            beside.append(push(3, 2 + 2 * pieces + q, whole_out.at[:, at], whole_out.at[:, at], mate))
-            put(0, whole_out.at[:, at], input_grad.at[:, at])
-            if q == pieces - 2:
-                finish_rows()
+            whole_out[:, lanes(q)] = (h_out[q].astype(F32) + h_in[q].astype(F32)).astype(BF16)
+            finish(q, q)
+        finish_rows()
+        gathered.wait_recv()
+        finish(3, theirs)
 
         for w in range(3):
             for k in (1, 2, 3) if mid else (1, 3):
@@ -466,16 +491,18 @@
         sent_all(part.at[pl.ds(1, 3)], d_send.at[0])
         if mid:
             sent_all(d_pass.at[pl.ds(2, 2)], e_send.at[0])
-        for i, ref in enumerate((f_out, g_out, h_out, whole_out.at[:, pl.ds(0, half)])):
+        for i, ref in enumerate((
+            f_out, g_out, x_out, h_out, whole_out.at[:, pl.ds(0, half)], whole_out.at[:, pl.ds(0, size)],
+        )):
             sent_all(ref, g_send.at[i])
         sent_all(n_in, n_send.at[0])
         for copy in swaps:
             copy.wait_send()
 
-        for q in range(pieces):
-            beside[q].wait_recv()
-            at = cols((1 - c) * half + q * size, size)
-            put(0, whole_out.at[:, at], input_grad.at[:, at])
+        for i, q in ((2, mine), (0, 0), (1, 1), (3, theirs)):
+            beside[i].wait_recv()
+            part_in = lanes(q, 1 - c)
+            put(0, whole_out.at[:, part_in], input_grad.at[:, part_in])
         for i, (src, dst) in enumerate(((whole_out, input_grad), (down_grad, down_grad), (n_sum, norms))):
             pltpu.make_async_copy(src, dst, out_sem.at[i]).wait()
 
@@ -502,8 +529,7 @@
     anywhere = pl.BlockSpec(memory_space=pl.ANY)
     vmem = pl.BlockSpec(memory_space=pltpu.VMEM)
     dma = pltpu.SemaphoreType.DMA
-    n, half, pieces = 4, depth // 2, 4
-    piece = (pieces, rows, half // pieces)
+    n, half, size = 4, depth // 2, depth // 8
     peers = 2 * n - 1
     scratch = [((2 * sub_m, depth), BF16)] * 3 + [((2 * sub_e, depth), BF16)] * 3
     scratch += [((2 * rows, depth), BF16), ((4 * rows, depth), BF16)]
@@ -512,7 +538,8 @@
         scratch += [((4 * rows, sub), BF16), ((2 * rows, sub), BF16)]
     scratch += [((n, sub_m, width), BF16), ((n, sub_e, width), BF16), ((sub_m, width), F32)]
     scratch += [((n, sub_m, width), BF16)] + [((n, sub_e, width), BF16)] * 2
-    scratch += [((2, rows, half), BF16)] * 2 + [(piece, F32)] + [(piece, BF16)] * 4
+    scratch += [((2, rows, half), BF16)] * 2 + [((4, rows, size), F32)]
+    scratch += [((3, rows, size), BF16)] * 2 + [((2, rows, size), BF16)] * 4
     scratch += [((rows, depth), BF16)] + [((sub_m, width), BF16), ((sub_e, width), BF16)] * 2
     scratch += [((8, both // 2), F32), ((peers, 8, both // 2), F32), ((8, both), F32)]
     input_grad, down_grad, norms = pl.pallas_call(
@@ -526,7 +553,7 @@
         out_specs=[anywhere] * 3,
         scratch_shapes=[pltpu.VMEM(shape, kind) for shape, kind in scratch] + [
             dma((count,)) for count in (
-                5, 9, 18, 3, 3, 3, 9, 9, 1, 12, 1, 1, 1, 3, 1, 2, 4, 2 + 3 * pieces, 2, 2, 1, 1, 3,
+                5, 9, 18, 3, 3, 3, 9, 9, 1, 12, 1, 1, 1, 3, 1, 2, 6, 14, 2, 2, 1, 1, 3,
             )
         ],
         compiler_params=pltpu.CompilerParams(collective_id=0, has_side_effects=True),

time: 91 us -> 87.3 us (0.959)
  Pallas kernels: 90.2 us -> 86.5 us
    pallas_call x1, Pallas kernels: 87.2 us -> 83.5 us  [split_units(): pl.pallas_call(block_kernel, out_shape=[jax.ShapeDtypeStruct((rows, depth...]
where the time goes in v5:
time: 87.3 us; the launch traced here: 87.2 us
  Pallas kernels  86.5 us (99%)
    pallas_call x1, Pallas kernels, split_units(): pl.pallas_call(block_kernel, out_shape=[jax.ShapeDtypeStruct((rows, depth...  83.5 us
    pallas_call x1, Pallas kernels, split_units(): pl.pallas_call(write_kernel, out_shape=[jax.ShapeDtypeStruct((rows, depth...  3.01 us

profile of v5, /device:TPU:0, one launch (start us, length us, event | category | flops | bytes accessed | tf_op | source)
XLA Modules:
  0.0 87.2 jit_solution(2408885262155694621)
XLA Ops:
  0.6 83.5 %block.1 = (bf16[256,2048]{1,0:T(8,128)(2,1)}, bf16[704,512]{1,0:T(8,128)(2,1)}, f32[8,704]{1,0:T(8,128)}) custom-call(bf16[704,512]{1,0:T(8,128)(2,1)} %bitcast.2, bf16[704,512]{1,0:T(8,128)(2,1)} %bitcast.3, bf16[704,512]{1,0:T(8,128)(2,1)} %down.1, bf16[256,2048]{1,0:T(8,128)(2,1)} %tokens.1, bf16[256,2048]{1,0:T(8,128)(2,1)} %grad.1), custom_call_target="tpu_custom_call" | custom-call | tf_op jit(solution)/shard_map/block/pallas_call | solution.py:545
  84.2 3.0 %write.1 = (bf16[256,2048]{1,0:T(8,128)(2,1)}, f32[704,512]{1,0:T(8,128)}, f32[704]{0:T(1024)}) custom-call(bf16[256,2048]{1,0:T(8,128)(2,1)} %get-tuple-element.6.flow, bf16[704,512]{1,0:T(8,128)(2,1)} %get-tuple-element.7.shard, f32[8,704]{1,0:T(8,128)} %get-tuple-element.8.rows), custom_call_target="tpu_custom_call" | custom-call | tf_op jit(solution)/shard_map/write/pallas_call | solution.py:562

commit v6 on v5

--- a/solution.py
+++ b/solution.py
@@ -23,7 +23,7 @@
     gate_m, up_m, down_m, gate_e, up_e, down_e, tokens_all, grad_all,
     gate_pre, up_pre, hid, gate_grad, up_grad, hid_all_m, hid_out_m, hid_all_e, hid_out_e,
     part_m, part_e, part_own, d_in_m, d_in_e, d_pass,
-    f_out, f_in, g_own, g_out, g_in, x_out, x_in, h_out, h_in, whole_out, s_own_m, s_own_e, s_other_m, s_other_e,
+    f_out, f_in, g_own, g_out, g_in, x_out, x_in, h_out, h_in, whole_out, s_own_m, s_own_e,
     n_own, n_in, n_sum,
     own_sem, w_send, w_recv, w_pass, b_send, b_recv, y_send, y_recv, t_send, t_recv, hid_send, hid_recv,
     d_send, d_recv, e_send, e_recv, g_send, g_recv, s_send, s_recv, n_send, n_recv, out_sem,
@@ -279,8 +279,9 @@
             pltpu.make_async_copy(src, dst, out_sem.at[group]).start()
 
         swaps = [
-            remote(own, theirs, s_send.at[i], s_recv.at[i], pair)
-            for i, (own, theirs) in enumerate(((s_own_m, s_other_m), (s_own_e, s_other_e)))
+            remote(own, down_grad.at[tile(bases[of] + r * subs[of], subs[of])],
+                   s_send.at[i], s_recv.at[i], pair)
+            for i, (of, own) in enumerate(((True, s_own_m), (False, s_own_e)))
         ]
         sums = {}
 
@@ -322,8 +323,6 @@
             put(2, n_sum, norms)
             for copy in swaps:
                 copy.wait_recv()
-            for of, theirs in ((True, s_other_m), (False, s_other_e)):
-                put(1, theirs, down_grad.at[tile(bases[of] + (1 - r) * subs[of], subs[of])])
 
         if mid:
             fetch(2).start()
@@ -446,11 +445,14 @@
         reduced[0].wait_recv()
         g_own[2] += x_in[0].astype(F32)
         sent = []
+        if not mid:
+            rows_of(True)
+            swaps[0].start()
         for q in range(2):
             over[q].wait_recv()
             h_out[q] = (g_own[q] + g_in[q].astype(F32)).astype(BF16)
             sent.append(push(3, 7 + q, h_out.at[q], h_in.at[q], far))
-            if q == 0:
+            if q == 0 and mid:
                 rows_of(True)
                 swaps[0].start()
         if not mid:
@@ -459,7 +461,7 @@
 
         def finish(i, q):
             part_out = whole_out.at[:, lanes(q)]
-            beside[i] = push(4, 10 + i, part_out, part_out, mate)
+            beside[i] = push(4, 10 + i, part_out, input_grad.at[:, lanes(q)], mate)
             put(0, part_out, input_grad.at[:, lanes(q)])
 
         over[2].wait_recv()
@@ -499,11 +501,13 @@
         for copy in swaps:
             copy.wait_send()
 
-        for i, q in ((2, mine), (0, 0), (1, 1), (3, theirs)):
+        for i in range(4):
             beside[i].wait_recv()
-            part_in = lanes(q, 1 - c)
-            put(0, whole_out.at[:, part_in], input_grad.at[:, part_in])
-        for i, (src, dst) in enumerate(((whole_out, input_grad), (down_grad, down_grad), (n_sum, norms))):
+        for i, (src, dst) in enumerate((
+            (whole_out.at[:, pl.ds(0, half)], input_grad.at[:, pl.ds(0, half)]),
+            (down_grad.at[pl.ds(0, sub_m + sub_e)], down_grad.at[pl.ds(0, sub_m + sub_e)]),
+            (n_sum, norms),
+        )):
             pltpu.make_async_copy(src, dst, out_sem.at[i]).wait()
 
     @pl.when(middle)
@@ -540,7 +544,7 @@
     scratch += [((n, sub_m, width), BF16)] + [((n, sub_e, width), BF16)] * 2
     scratch += [((2, rows, half), BF16)] * 2 + [((4, rows, size), F32)]
     scratch += [((3, rows, size), BF16)] * 2 + [((2, rows, size), BF16)] * 4
-    scratch += [((rows, depth), BF16)] + [((sub_m, width), BF16), ((sub_e, width), BF16)] * 2
+    scratch += [((rows, depth), BF16)] + [((sub_m, width), BF16), ((sub_e, width), BF16)]
     scratch += [((8, both // 2), F32), ((peers, 8, both // 2), F32), ((8, both), F32)]
     input_grad, down_grad, norms = pl.pallas_call(
         block_kernel,

time: 87.3 us -> 86.9 us (level)
  no operation moved by 1% of the time
where the time goes in v6:
time: 86.9 us; the launch traced here: 86.7 us
  Pallas kernels  86.1 us (99%)
    pallas_call x1, Pallas kernels, split_units(): pl.pallas_call(block_kernel, out_shape=[jax.ShapeDtypeStruct((rows, depth...  83 us
    pallas_call x1, Pallas kernels, split_units(): pl.pallas_call(write_kernel, out_shape=[jax.ShapeDtypeStruct((rows, depth...  3.01 us

profile of v6, /device:TPU:0, one launch (start us, length us, event | category | flops | bytes accessed | tf_op | source)
XLA Modules:
  0.0 86.7 jit_solution(6880166499193885624)
XLA Ops:
  0.6 83.0 %block.1 = (bf16[256,2048]{1,0:T(8,128)(2,1)}, bf16[704,512]{1,0:T(8,128)(2,1)}, f32[8,704]{1,0:T(8,128)}) custom-call(bf16[704,512]{1,0:T(8,128)(2,1)} %bitcast.2, bf16[704,512]{1,0:T(8,128)(2,1)} %bitcast.3, bf16[704,512]{1,0:T(8,128)(2,1)} %down.1, bf16[256,2048]{1,0:T(8,128)(2,1)} %tokens.1, bf16[256,2048]{1,0:T(8,128)(2,1)} %grad.1), custom_call_target="tpu_custom_call" | custom-call | tf_op jit(solution)/shard_map/block/pallas_call | solution.py:549
  83.7 3.0 %write.1 = (bf16[256,2048]{1,0:T(8,128)(2,1)}, f32[704,512]{1,0:T(8,128)}, f32[704]{0:T(1024)}) custom-call(bf16[256,2048]{1,0:T(8,128)(2,1)} %get-tuple-element.6.flow, bf16[704,512]{1,0:T(8,128)(2,1)} %get-tuple-element.7.shard, f32[8,704]{1,0:T(8,128)} %get-tuple-element.8.rows), custom_call_target="tpu_custom_call" | custom-call | tf_op jit(solution)/shard_map/write/pallas_call | solution.py:566

commit v7 on v6

--- a/solution.py
+++ b/solution.py
@@ -130,8 +130,6 @@
         whole = wholes[mid]
         hid_all, hid_out, part = (hid_all_m, hid_out_m, part_m) if mid else (hid_all_e, hid_out_e, part_e)
         role = (mid, not mid, not mid, mid)
-        for copy in own_rows(mid):
-            copy.start()
 
         def strip(w, j):
             size = width // cuts[w]
@@ -159,7 +157,7 @@
         def across(w, k, j):
             return remote(
                 whole[w].at[pl.ds(0, sub), place(w, k, j)], whole[w].at[pl.ds(sub, sub), place(w, k, j)],
-                y_send.at[3 * w + k - 1], y_recv.at[3 * w + k - 1], pair,
+                y_send.at[w], y_recv.at[3 * w + k - 1], pair,
             )
 
         def give(w, k):
@@ -332,6 +330,8 @@
             give(0, 1)
             fetch(1).start()
             give(1, 1)
+            for copy in own_rows(mid):
+                copy.start()
             arrive(0, 1)
             give(0, 2)
             arrive(0, 3)
@@ -378,6 +378,8 @@
             give(2, 1)
             give(2, 3)
             give_second(2)
+            for copy in own_rows(mid):
+                copy.start()
             hand(2)
             hand(0)
             arrive(0, 1)
@@ -482,12 +484,12 @@
             for k in (1, 2, 3) if mid else (1, 3):
                 weight(w, k, None).wait_send()
             (relay if mid else second)(w, None).wait_send()
-            for k in (2, 3) if mid else (1, 2, 3):
-                across(w, k, None).wait_send()
 
         def sent_all(ref, sem):
             remote(ref, ref, sem, sem, pair).wait_send()
 
+        for w in range(3):
+            sent_all(whole[w].at[pl.ds(0, sub), pl.ds(0, (2 if mid else 3) * width)], y_send.at[w])
         sent_all(grad_all, t_send.at[0])
         hid_swap.wait_send()
         sent_all(part.at[pl.ds(1, 3)], d_send.at[0])
@@ -557,7 +559,7 @@
         out_specs=[anywhere] * 3,
         scratch_shapes=[pltpu.VMEM(shape, kind) for shape, kind in scratch] + [
             dma((count,)) for count in (
-                5, 9, 18, 3, 3, 3, 9, 9, 1, 12, 1, 1, 1, 3, 1, 2, 6, 14, 2, 2, 1, 1, 3,
+                5, 9, 18, 3, 3, 3, 3, 9, 1, 12, 1, 1, 1, 3, 1, 2, 6, 14, 2, 2, 1, 1, 3,
             )
         ],
         compiler_params=pltpu.CompilerParams(collective_id=0, has_side_effects=True),

time: 86.9 us -> 86.8 us (level)
  no operation moved by 1% of the time
where the time goes in v7:
time: 86.8 us; the launch traced here: 86.6 us
  Pallas kernels  86 us (99%)
    pallas_call x1, Pallas kernels, split_units(): pl.pallas_call(block_kernel, out_shape=[jax.ShapeDtypeStruct((rows, depth...  83 us
    pallas_call x1, Pallas kernels, split_units(): pl.pallas_call(write_kernel, out_shape=[jax.ShapeDtypeStruct((rows, depth...  3.01 us

profile of v7, /device:TPU:0, one launch (start us, length us, event | category | flops | bytes accessed | tf_op | source)
XLA Modules:
  0.0 86.6 jit_solution(18114340647307701163)
XLA Ops:
  0.6 83.0 %block.1 = (bf16[256,2048]{1,0:T(8,128)(2,1)}, bf16[704,512]{1,0:T(8,128)(2,1)}, f32[8,704]{1,0:T(8,128)}) custom-call(bf16[704,512]{1,0:T(8,128)(2,1)} %bitcast.2, bf16[704,512]{1,0:T(8,128)(2,1)} %bitcast.3, bf16[704,512]{1,0:T(8,128)(2,1)} %down.1, bf16[256,2048]{1,0:T(8,128)(2,1)} %tokens.1, bf16[256,2048]{1,0:T(8,128)(2,1)} %grad.1), custom_call_target="tpu_custom_call" | custom-call | tf_op jit(solution)/shard_map/block/pallas_call | solution.py:551
  83.6 3.0 %write.1 = (bf16[256,2048]{1,0:T(8,128)(2,1)}, f32[704,512]{1,0:T(8,128)}, f32[704]{0:T(1024)}) custom-call(bf16[256,2048]{1,0:T(8,128)(2,1)} %get-tuple-element.6.flow, bf16[704,512]{1,0:T(8,128)(2,1)} %get-tuple-element.7.shard, f32[8,704]{1,0:T(8,128)} %get-tuple-element.8.rows), custom_call_target="tpu_custom_call" | custom-call | tf_op jit(solution)/shard_map/write/pallas_call | solution.py:568
